TPU v7x, 32 devices: a whole 2x2x4 slice. The times are simulated.
32 devices in a mesh: rep: 2 (over x), fs: 4 (over z), tp: 4 (over y, core).
Axes of the slice: x: 2, y: 2, z: 4, core: 2. Of those that a mesh axis runs over, the one named last changes fastest.
Arguments:
- tokens: bfloat16 [4096, 2048], P(('rep', 'fs', 'tp')), may hold values from -6 to 6
- mixer_gain: float32 [2048], replicated, may hold values from 0.1 to 1.9
- direct_weight: float32 [2048, 1024], P('fs', 'tp'), may hold values from -0.125 to 0.125
- direct_scale: float32 [1024], P('tp'), may hold values from 0.5 to 2
- value_weight: float32 [2048, 1024], P('fs', 'tp'), may hold values from -0.125 to 0.125
- value_scale: float32 [1024], P('tp'), may hold values from 0.5 to 8, as said below
- value_gain: float32 [1024], P('tp'), may hold values from 0.1 to 1.9
- value_shift: float32 [1024], P('tp'), may hold values from -3 to 3
- spatial_weight: bfloat16 [16, 128, 128], P('tp'), may hold values from -0.25 to 0.25
- spatial_bias: float32 [16, 128], P('tp'), may hold values from 0.1 to 1.9
- merge_weight: float32 [1024, 2048], P('tp', 'fs'), may hold values from -0.1875 to 0.1875
- merge_scale: float32 [2048], P('fs'), may hold values from 0.5 to 2
- channel_gain: float32 [2048], replicated, may hold values from 0.1 to 1.9
- expand_weight: float32 [2048, 8192], P('fs', 'tp'), may hold values from -0.125 to 0.125
- expand_scale: float32 [8192], P('tp'), may hold values from 0.5 to 2
- reduce_weight: float32 [8192, 2048], P('tp', 'fs'), may hold values from -0.0625 to 0.0625
- reduce_scale: float32 [2048], P('fs'), may hold values from 0.5 to 2
Outputs:
- result: bfloat16 [4096, 2048], P(('rep', 'fs', 'tp'))
Inputs may be any that keep to these rules, and one draw needn't show every extreme that they name: `value_scale`: positive column scales.
All inputs are finite; a program needn't handle non-finite values.
Results may differ from a plain program's by a relative error of at most 0.024.
Values may be sent and summed in bfloat16 or wider, within the bound.
A program may use at most 64 MiB of HBM per device.

v0:
```python
import jax
import jax.numpy as jnp
from jax import lax
from jax.experimental import pallas as pl
from jax.experimental.pallas import tpu as pltpu
from jax.sharding import PartitionSpec as P

GDIM = 64
BLOCK = 128


epsilon = 1e-06


def rms_rows(rows, gain):
    floats = rows.astype(jnp.float32)
    scaled = floats * lax.rsqrt(jnp.mean(floats * floats, axis=-1, keepdims=True) + epsilon)
    return (scaled * gain).astype(jnp.bfloat16)


def body(
    tokens,
    mixer_gain,
    direct_weight,
    direct_scale,
    value_weight,
    value_scale,
    value_gain,
    value_shift,
    spatial_weight,
    spatial_bias,
    merge_weight,
    merge_scale,
    channel_gain,
    expand_weight,
    expand_scale,
    reduce_weight,
    reduce_scale,
):
    direct_half = direct_weight.astype(jnp.bfloat16)
    value_half = value_weight.astype(jnp.bfloat16)
    merge_half = merge_weight.astype(jnp.bfloat16)
    expand_half = expand_weight.astype(jnp.bfloat16)
    reduce_half = reduce_weight.astype(jnp.bfloat16)
    full_expand, full_reduce, reduce_full_scale = (
        lax.all_gather(expand_half, "fs", axis=0, tiled=True),
        lax.all_gather(reduce_half, "fs", axis=1, tiled=True),
        lax.all_gather(reduce_scale.astype(jnp.bfloat16), "fs", axis=0, tiled=True).astype(
            reduce_scale.dtype
        ),
    )
    normed = rms_rows(tokens, mixer_gain)
    whole = lax.all_gather(normed, "tp", axis=0, tiled=True)
    seq_rows = whole.shape[0]
    local_width = direct_weight.shape[1]
    direct_pre = jnp.dot(
        whole,
        lax.all_gather(direct_half, "fs", axis=0, tiled=True),
        preferred_element_type=jnp.float32,
    )
    value_pre = jnp.dot(
        whole,
        lax.all_gather(value_half, "fs", axis=0, tiled=True),
        preferred_element_type=jnp.float32,
    )
    full_merge, merge_full_scale = (
        lax.all_gather(merge_half, "fs", axis=1, tiled=True),
        lax.all_gather(merge_scale.astype(jnp.bfloat16), "fs", axis=0, tiled=True).astype(
            merge_scale.dtype
        ),
    )
    direct = jax.nn.gelu(direct_pre * direct_scale)
    value = jax.nn.gelu(value_pre * value_scale)
    total, squares = lax.psum((jnp.sum(value, axis=1), jnp.sum(value * value, axis=1)), "tp")
    branch_width = local_width * lax.axis_size("tp")
    mean = (total / branch_width)[:, None]
    var = (squares / branch_width)[:, None] - mean * mean
    gated_value = ((value - mean) * lax.rsqrt(var + epsilon) * value_gain + value_shift).astype(
        jnp.bfloat16
    )
    local_groups = spatial_weight.shape[0]
    blocks = gated_value.reshape(seq_rows // BLOCK, BLOCK, local_groups, GDIM)
    mixed = jnp.einsum("gpq,nqgc->npgc", spatial_weight, blocks, preferred_element_type=jnp.float32)
    mixed = mixed + jnp.transpose(spatial_bias)[None, :, :, None]
    gated = (direct * mixed.reshape(seq_rows, local_width)).astype(jnp.bfloat16)
    rows = gated
    mix = lax.psum_scatter(
        (jnp.dot(rows, full_merge, preferred_element_type=jnp.float32) * merge_full_scale).astype(
            jnp.bfloat16
        ),
        "tp",
        scatter_dimension=0,
        tiled=True,
    ).astype(jnp.float32)
    middle = (tokens.astype(jnp.float32) + mix).astype(jnp.bfloat16)
    normed_mid = rms_rows(middle, channel_gain)
    whole_mid = lax.all_gather(normed_mid, "tp", axis=0, tiled=True)
    upper = jnp.dot(whole_mid, full_expand, preferred_element_type=jnp.float32)
    hidden = jnp.square(jax.nn.relu(upper * expand_scale)).astype(jnp.bfloat16)
    rows = hidden
    lower = lax.psum_scatter(
        (jnp.dot(rows, full_reduce, preferred_element_type=jnp.float32) * reduce_full_scale).astype(
            jnp.bfloat16
        ),
        "tp",
        scatter_dimension=0,
        tiled=True,
    ).astype(jnp.float32)
    return (middle.astype(jnp.float32) + lower).astype(jnp.bfloat16)


MESH = pl.DeviceIdType.MESH


def fused_kernel(
    tok_ref, mgain_ref, dv_ref, dvscale_ref, vgain_ref, vshift_ref, sw_ref, sbias_ref,
    mg_ref, cgain_ref, ex_ref, exscale_ref, rd_ref,
    out_ref,
    dv_all, mg_all, ex_all, rd_all,
    xg, act, stat, gated, p1, r1, s1, x1, mid,
    nm, acc, hid, p2, r2, s2, z2, s3, x2,
    own_sem, wsend, wrecv, xsend, xrecv, gsend, grecv, tsend, trecv, msend, mrecv, nsend, nrecv, fsend, frecv,
):
    rows, width = tok_ref.shape
    piece = dv_ref.shape[0]
    local = vgain_ref.shape[1]
    seq = xg.shape[0]
    r = lax.axis_index("rep")
    f = lax.axis_index("fs")
    t = lax.axis_index("tp")
    y, c = t // 2, t % 2
    z = f % 2
    mate = f + 1 - 2 * z
    peers = (mate, (f + 2) % 4, (mate + 2) % 4)
    sib = {"tp": y * 2 + (1 - c)}
    ynb = {"tp": (1 - y) * 2 + c}
    xnb = {"rep": 1 - r}
    znb = {"fs": mate}

    barrier = pltpu.get_barrier_semaphore()
    for dev in (sib, ynb, xnb) + tuple({"fs": peer} for peer in peers):
        pl.semaphore_signal(barrier, inc=1, device_id=dev, device_id_type=MESH)
    pl.semaphore_wait(barrier, 6)

    def rcopy(src, dst, ssem, rsem, dev):
        return pltpu.make_async_remote_copy(
            src_ref=src, dst_ref=dst, send_sem=ssem, recv_sem=rsem,
            device_id=dev, device_id_type=MESH,
        )

    mixer = ((dv_ref, dv_all), (mg_ref, mg_all))

    def part(i, slot, q):
        ref = mixer[i][1]
        size = ref.shape[1] // 2
        return ref.at[slot, pl.ds(pl.multiple_of(q * size, size), size)]

    def along(i, j):
        src = mixer[i][0]
        size = src.shape[0] // 2
        return rcopy(
            src.at[pl.ds(pl.multiple_of(r * size, size), size)], part(i, f, r),
            wsend.at[i, j], wrecv.at[i, j], {"fs": peers[j]},
        )

    def over(i, j):
        here = part(i, peers[j], r)
        return rcopy(here, here, xsend.at[i, j], xrecv.at[i, j], xnb)

    def over_start(i):
        for j in range(3):
            along(i, j).wait_recv()
            over(i, j).start()

    def over_wait(i):
        for j in range(3):
            over(i, j).wait_recv()

    def chunk(i, j):
        to = peers[j] % 2
        src = ex_ref.at[to] if i == 2 else rd_ref.at[to, i - 3]
        dst = ex_all.at[f] if i == 2 else rd_all.at[f, i - 3]
        return rcopy(src, dst, wsend.at[i, j], wrecv.at[i, j], {"fs": peers[j]})

    for i in range(2):
        for j in range(3):
            along(i, j).start()
    for j in range(3):
        chunk(2, j).start()
    owns = [
        pltpu.make_async_copy(src, dst.at[f], own_sem.at[i])
        for i, (src, dst) in enumerate(
            mixer + ((ex_ref.at[z], ex_all), (rd_ref.at[z], rd_all))
        )
    ]
    for own in owns:
        own.start()

    def norm(x, gain):
        return (
            x * lax.rsqrt(jnp.mean(x * x, axis=-1, keepdims=True) + epsilon) * gain
        ).astype(jnp.bfloat16)

    def block(n, size=1):
        return pl.ds(pl.multiple_of(n * rows, rows), size * rows)

    def columns(slot):
        return pl.ds(pl.multiple_of(slot * piece, piece), piece)

    mine = xg.at[block(c * 2 + y)]
    mine[...] = norm(tok_ref[...].astype(jnp.float32), mgain_ref[...])
    far = xg.at[block(c * 2 + 1 - y)]
    gather = (
        rcopy(mine, mine, gsend.at[0], grecv.at[0], sib),
        rcopy(mine, mine, gsend.at[1], grecv.at[1], ynb),
        rcopy(far, far, gsend.at[2], grecv.at[2], sib),
    )
    gather[1].start()
    gather[0].start()
    gather[1].wait_recv()
    gather[2].start()
    over_start(0)
    over_start(1)
    gather[0].wait_recv()
    gather[2].wait_recv()
    for own in owns:
        own.wait()

    def project(slot):
        return jnp.dot(xg[:, columns(slot)], dv_all[slot], preferred_element_type=jnp.float32)

    over_wait(0)
    act[...] = project(f)
    for peer in peers:
        act[...] += project(peer)
    act[...] = jax.nn.gelu(act[...] * dvscale_ref[...])

    lane = lax.broadcasted_iota(jnp.int32, (rows, rows), 1)
    for n in range(4):
        value = act[n * rows : (n + 1) * rows, local:]
        total = jnp.sum(value, axis=1, keepdims=True)
        squares = jnp.sum(value * value, axis=1, keepdims=True)
        table = jnp.where(lane == 0, total, jnp.where(lane == 1, squares, 0.0))
        stat[t, n] = jnp.transpose(table)[:8]
    stats = [
        rcopy(stat.at[t], stat.at[t], tsend.at[0], trecv.at[0], sib),
        rcopy(stat.at[t], stat.at[t], tsend.at[1], trecv.at[1], ynb),
        rcopy(
            stat.at[(1 - y) * 2 + c], stat.at[(1 - y) * 2 + c], tsend.at[2], trecv.at[2], sib
        ),
    ]
    stats[1].start()
    stats[0].start()
    stats[1].wait_recv()
    stats[2].start()
    stats[0].wait_recv()
    stats[2].wait_recv()
    inverse = 1.0 / (local * 4)
    group_lane = lax.broadcasted_iota(jnp.int32, (rows, 128), 1) // GDIM
    for n in range(4):
        here = slice(n * rows, (n + 1) * rows)
        summed = stat[0, n] + stat[1, n] + stat[2, n] + stat[3, n]
        table = jnp.transpose(jnp.concatenate([summed] * (rows // 8), axis=0))
        mean = table[:, 0:1] * inverse
        var = table[:, 1:2] * inverse - mean * mean
        gv = (
            (act[here, local:] - mean) * lax.rsqrt(var + epsilon) * vgain_ref[...]
            + vshift_ref[...]
        ).astype(jnp.bfloat16)
        per = 128 // GDIM
        for j in range(local // 128):
            at = slice(j * 128, (j + 1) * 128)
            mixed = jnp.dot(sw_ref[j * per], gv[:, at], preferred_element_type=jnp.float32)
            for k in range(1, per):
                other = jnp.dot(
                    sw_ref[j * per + k], gv[:, at], preferred_element_type=jnp.float32
                )
                mixed = jnp.where(group_lane == k, other, mixed)
            gated[here, at] = (act[here, at] * (mixed + sbias_ref[:, at])).astype(jnp.bfloat16)

    slots = (f,) + peers

    def merge_pair(k):
        return rcopy(
            p1.at[k, block((1 - c) * 2, 2)], r1.at[k], msend.at[k, 0], mrecv.at[k, 0], sib
        )

    def merge_far(k):
        return rcopy(s1.at[k], x1.at[k], msend.at[k, 1], mrecv.at[k, 1], ynb)

    def merge_send(k):
        merge_pair(k).wait_recv()
        s1[k] = (
            p1[k, block(c * 2 + 1 - y)].astype(jnp.float32)
            + r1[k, block(1 - y)].astype(jnp.float32)
        ).astype(jnp.bfloat16)
        merge_far(k).start()

    for k, slot in enumerate(slots):
        if k == 1:
            over_wait(1)
        p1[k] = jnp.dot(gated[...], mg_all[slot], preferred_element_type=jnp.float32).astype(
            jnp.bfloat16
        )
        merge_pair(k).start()
        if k > 0:
            merge_send(k - 1)
    merge_send(3)
    for k, slot in enumerate(slots):
        merge_far(k).wait_recv()
        mid[:, columns(slot)] = (
            tok_ref[:, columns(slot)].astype(jnp.float32)
            + p1[k, block(c * 2 + y)].astype(jnp.float32)
            + r1[k, block(y)].astype(jnp.float32)
            + x1[k].astype(jnp.float32)
        ).astype(jnp.bfloat16)

    def place(zz, rr, yy):
        return nm.at[block(c * 8 + zz * 4 + rr * 2 + yy)]

    half = rows // 2
    mine = place(z, r, y)
    mine[...] = norm(mid[...].astype(jnp.float32), cgain_ref[...])
    over_fs = rcopy(mine, mine, nsend.at[16], nrecv.at[16], znb)

    def spreading(b, zz):
        here = place(zz, r, y)
        from_x, from_y = place(zz, 1 - r, y), place(zz, r, 1 - y)
        from_xy = place(zz, 1 - r, 1 - y)
        low, high = from_x.at[pl.ds(0, half)], from_y.at[pl.ds(half, half)]
        routes = (
            (here, xnb), (here, ynb), (here, sib), (low, ynb), (high, xnb),
            (from_x, sib), (from_y, sib), (from_xy, sib),
        )
        return tuple(
            rcopy(ref, ref, nsend.at[8 * b + k], nrecv.at[8 * b + k], dev)
            for k, (ref, dev) in enumerate(routes)
        )

    near, far = spreading(0, z), spreading(1, 1 - z)
    over_fs.start()
    for i in range(3, 5):
        for j in range(3):
            chunk(i, j).start()
    for k in range(3):
        near[k].start()
    over_fs.wait_recv()
    for k in range(3):
        far[k].start()
    for spread in (near, far):
        for k in range(2):
            spread[k].wait_recv()
            spread[3 + k].start()
            spread[5 + k].start()
    for spread in (near, far):
        spread[3].wait_recv()
        spread[4].wait_recv()
        spread[7].start()
    for spread in (near, far):
        for k in (2, 5, 6, 7):
            spread[k].wait_recv()

    everyone = nm.shape[0]
    tall = 2 * rows

    def over_rows(step):
        lax.fori_loop(
            0, everyone // tall,
            lambda i, _: step(pl.ds(pl.multiple_of(i * tall, tall), tall)), None,
        )

    def expand(at, slot):
        return jnp.dot(nm[at, columns(slot)], ex_all[slot], preferred_element_type=jnp.float32)

    def expand_most(at):
        acc[at] = expand(at, f) + expand(at, peers[0])

    def expand_last(at):
        upper = (acc[at] + expand(at, peers[1]) + expand(at, peers[2])) * exscale_ref[...]
        hid[at] = jnp.square(jax.nn.relu(upper)).astype(jnp.bfloat16)

    chunk(2, 0).wait_recv()
    over_rows(expand_most)
    chunk(2, 1).wait_recv()
    chunk(2, 2).wait_recv()
    over_rows(expand_last)

    def down_pair(k):
        return rcopy(
            p2.at[k, block((1 - c) * 8, 8)], r2.at[k], fsend.at[k, 0], frecv.at[k, 0], sib
        )

    def down_fs(k):
        return rcopy(
            s2.at[k], z2.at[k], fsend.at[k, 7], frecv.at[k, 7], znb
        )

    def down_fs_send(k):
        down_pair(k).wait_recv()
        s2[k] = (
            p2[k, block(c * 8 + (1 - z) * 4, 4)].astype(jnp.float32)
            + r2[k, block((1 - z) * 4, 4)].astype(jnp.float32)
        ).astype(jnp.bfloat16)
        down_fs(k).start()

    hops = ((1 - r, y), (r, 1 - y), (1 - r, 1 - y))

    def down_far(k, h):
        rr, yy = hops[h]
        dev = (xnb, ynb)[h]
        return rcopy(
            s3.at[k, block(rr * 2 + yy)], x2.at[k, h], fsend.at[k, 1 + h], frecv.at[k, 1 + h], dev
        )

    def down_via(k, h):
        return rcopy(
            s3.at[k, pl.ds(pl.multiple_of((hops[2][0] * 2 + hops[2][1]) * rows + h * half, half), half)],
            x2.at[k, 2, pl.ds(h * half, half)],
            fsend.at[k, 3 + h], frecv.at[k, 3 + h], (xnb, ynb)[h],
        )

    def down_on(k, h):
        return rcopy(
            x2.at[k, 2, pl.ds(h * half, half)], x2.at[k, 3, pl.ds(h * half, half)],
            fsend.at[k, 5 + h], frecv.at[k, 5 + h], (ynb, xnb)[h],
        )

    def down_send(k):
        down_fs(k).wait_recv()
        s3[k] = (
            p2[k, block(c * 8 + z * 4, 4)].astype(jnp.float32)
            + r2[k, block(z * 4, 4)].astype(jnp.float32)
            + z2[k].astype(jnp.float32)
        ).astype(jnp.bfloat16)
        for h in range(2):
            down_via(k, h).start()
        for h in range(2):
            down_far(k, h).start()

    def down_relay(k):
        for h in range(2):
            down_via(k, h).wait_recv()
            down_on(k, h).start()

    steps = ((0, 0), (1, 0), (0, 1), (1, 1), (2, 0), (3, 0), (2, 1), (3, 1))
    base = f - z
    order = (base, base + 1, 2 - base, 3 - base)

    def arrived(side, j):
        rcopy(
            rd_ref.at[0, side], rd_all.at[f, side],
            wsend.at[3 + side, j], wrecv.at[3 + side, j], znb,
        ).wait_recv()

    last = len(steps)
    thin = piece // 2

    for k in range(last + 3):
        if k < last:
            from_slot, side = steps[k]
            slot = order[from_slot]
            if from_slot == 0:
                arrived(side, 0)
            elif from_slot > 1:
                arrived(side, 1 + (from_slot + z) % 2)

            def reduce(at, k=k, slot=slot, side=side):
                p2[k, at] = jnp.dot(
                    hid[at], rd_all[slot, side], preferred_element_type=jnp.float32
                ).astype(jnp.bfloat16)

            over_rows(reduce)
            down_pair(k).start()
        if 0 < k <= last:
            down_fs_send(k - 1)
        if 1 < k <= last + 1:
            down_send(k - 2)
        if 2 < k:
            down_relay(k - 3)
    for k, (from_slot, side) in enumerate(steps):
        for h in range(2):
            down_far(k, h).wait_recv()
            down_on(k, h).wait_recv()
        at = pl.ds(pl.multiple_of(order[from_slot] * piece + side * thin, thin), thin)
        out_ref[:, at] = (
            mid[:, at].astype(jnp.float32)
            + p2[k, block(c * 8 + z * 4 + r * 2 + y)].astype(jnp.float32)
            + r2[k, block(z * 4 + r * 2 + y)].astype(jnp.float32)
            + z2[k, block(r * 2 + y)].astype(jnp.float32)
            + x2[k, 0].astype(jnp.float32)
            + x2[k, 1].astype(jnp.float32)
            + x2[k, 3].astype(jnp.float32)
        ).astype(jnp.bfloat16)

    for j in range(3):
        for i in range(2):
            along(i, j).wait_send()
            over(i, j).wait_send()
        for i in range(2, 5):
            chunk(i, j).wait_send()
    for copy in gather + tuple(stats) + near + far + (over_fs,):
        copy.wait_send()
    for k in range(4):
        merge_pair(k).wait_send()
        merge_far(k).wait_send()
    for k in range(last):
        down_pair(k).wait_send()
        down_fs(k).wait_send()
        for h in range(2):
            down_far(k, h).wait_send()
            down_via(k, h).wait_send()
            down_on(k, h).wait_send()


def fused_body(
    tokens,
    mixer_gain,
    direct_weight,
    direct_scale,
    value_weight,
    value_scale,
    value_gain,
    value_shift,
    spatial_weight,
    spatial_bias,
    merge_weight,
    merge_scale,
    channel_gain,
    expand_weight,
    expand_scale,
    reduce_weight,
    reduce_scale,
):
    bf = jnp.bfloat16
    rows, width = tokens.shape
    piece, local = direct_weight.shape
    wide = expand_weight.shape[1] // 2
    r = lax.axis_index("rep")
    unit = wide // 2
    f = lax.axis_index("fs")
    dv = jnp.concatenate([direct_weight.astype(bf), value_weight.astype(bf)], axis=1)
    dvscale = jnp.concatenate([direct_scale, value_scale])[None]
    sbias = jnp.repeat(jnp.transpose(spatial_bias), GDIM, axis=1)
    mg = (merge_weight * merge_scale).astype(bf)
    ex = lax.dynamic_slice_in_dim(expand_weight, r * wide, wide, 1).astype(bf)
    ex = jnp.stack([ex[:, :unit], ex[:, unit:]])
    exscale = lax.dynamic_slice_in_dim(expand_scale, r * wide + f % 2 * unit, unit, 0)[None]
    rd = (lax.dynamic_slice_in_dim(reduce_weight, r * wide, wide, 0) * reduce_scale).astype(bf)
    rd = jnp.transpose(rd.reshape(2, unit, 2, piece // 2), (0, 2, 1, 3))
    seq = 4 * rows
    vm = pltpu.VMEM
    dma = pltpu.SemaphoreType.DMA
    f32 = jnp.float32
    operands = (
        tokens, mixer_gain[None], dv, dvscale, value_gain[None], value_shift[None],
        spatial_weight, sbias, mg, channel_gain[None], ex, exscale, rd,
    )
    return pl.pallas_call(
        fused_kernel,
        out_shape=jax.ShapeDtypeStruct((rows, width), bf),
        in_specs=[pl.BlockSpec(memory_space=pltpu.VMEM)] * len(operands),
        out_specs=pl.BlockSpec(memory_space=pltpu.VMEM),
        scratch_shapes=[
            vm((4, piece, 2 * local), bf),
            vm((4, local, piece), bf),
            vm((4, piece, unit), bf),
            vm((4, 2, unit, piece // 2), bf),
            vm((seq, width), bf),
            vm((seq, 2 * local), f32),
            vm((4, 4, 8, rows), f32),
            vm((seq, local), bf),
            vm((4, seq, piece), bf),
            vm((4, 2 * rows, piece), bf),
            vm((4, rows, piece), bf),
            vm((4, rows, piece), bf),
            vm((rows, width), bf),
            vm((4 * seq, width), bf),
            vm((4 * seq, unit), f32),
            vm((4 * seq, unit), bf),
            vm((8, 4 * seq, piece // 2), bf),
            vm((8, 2 * seq, piece // 2), bf),
            vm((8, seq, piece // 2), bf),
            vm((8, seq, piece // 2), bf),
            vm((8, seq, piece // 2), bf),
            vm((8, 4, rows, piece // 2), bf),
            dma((4,)),
            dma((5, 3)), dma((5, 3)),
            dma((2, 3)), dma((2, 3)),
            dma((3,)), dma((3,)),
            dma((3,)), dma((3,)),
            dma((4, 2)), dma((4, 2)),
            dma((17,)), dma((17,)),
            dma((8, 8)), dma((8, 8)),
        ],
        compiler_params=pltpu.CompilerParams(
            collective_id=0, has_side_effects=True, vmem_limit_bytes=60 * 1024 * 1024
        ),
    )(*operands)


def solution(mesh):
    sizes = mesh.shape
    fused = sizes["rep"] == 2 and sizes["fs"] == 4 and sizes["tp"] == 4
    return jax.shard_map(
        fused_body if fused else body,
        mesh=mesh,
        in_specs=(
            P(("rep", "fs", "tp"), None),
            P(),
            P("fs", "tp"),
            P("tp"),
            P("fs", "tp"),
            P("tp"),
            P("tp"),
            P("tp"),
            P("tp", None, None),
            P("tp", None),
            P("tp", "fs"),
            P("fs"),
            P(),
            P("fs", "tp"),
            P("tp"),
            P("tp", "fs"),
            P("fs"),
        ),
        out_specs=P(("rep", "fs", "tp"), None),
        check_vma=False,
    )
```

profile of v0, /device:TPU:0, one launch (start us, length us, event | category | flops | bytes accessed | tf_op | source)
XLA Modules:
  0.0 189.7 jit_solution(1179295149455482999)
XLA Ops:
  0.0 0.0 copy-start.4
  0.0 1.4 dynamic_slice.10
  1.4 0.0 copy-start
  1.4 1.9 dynamic-slice_convert_fusion
  3.3 0.1 slice_bitcast_fusion.1
  3.3 1.1 pad_maximum_fusion.ex_ref
  4.4 0.0 copy-done.4
  4.4 0.0 copy-done
  4.4 0.0 copy-start.1
  4.4 0.0 copy-start.2
  4.4 0.3 multiply_convert_fusion
  4.7 0.0 copy-start.5
  4.7 0.0 copy-start.6
  4.7 0.0 copy-start.7
  4.8 0.0 copy-start.8
  4.8 0.3 reshape.9
  5.1 0.0 copy-start.3
  5.1 1.2 copy.22
  6.2 0.0 copy-done.1
  6.3 0.0 copy-done.2
  6.3 0.8 pad_maximum_fusion.1.dv_ref
  7.2 0.0 copy-done.5
  7.2 0.8 copy.20.sbias_ref
  7.9 0.0 copy-done.6
  7.9 0.0 copy-done.3
  7.9 0.7 multiply_convert_fusion.1.mg_ref
  8.7 0.0 copy-done.7
  8.7 0.0 copy-done.8
  8.7 0.6 pad_maximum_fusion.2
  9.3 178.5 %shard_map.163 = bf16[128,2048]{1,0:T(8,128)(2,1)} custom-call(bf16[128,2048]{1,0:T(8,128)(2,1)} %tok_ref.1, f32[1,2048]{1,0:T(1,128)} %bitcast.17, bf16[512,512]{1,0:T(8,128)(2,1)} %pad_maximum_fusion.1.dv_ref, f32[1,512]{1,0:T(1,128)} %bitcast.20, f32[1,256]{1,0:T(1,128)} %bitcast.22, f32[1,256]{1,0:T(1,128)} %bitcast.23, bf16[4,128,128]{2,1,0:T(8,128)(2,1)} %sw_ref.1, ...), custom_call_target="tpu_custom_call" | custom-call | tf_op jit(solution)/shard_map/pallas_call | solution.py:558
  187.8 1.9 copy.24
  (3 shorter events, 0.1 us)
Async XLA Ops:
  0.0 4.4 %copy-start.4 = (f32[512]{0:T(512)S(1)}, f32[512]{0:T(512)}, u32[]{:S(2)}) copy-start(f32[512]{0:T(512)} %param.33) | copy-start | bytes 6148
  1.4 3.0 %copy-start = (f32[2048,512]{1,0:T(8,128)S(1)}, f32[2048,512]{1,0:T(8,128)}, u32[]{:S(2)}) copy-start(f32[2048,512]{1,0:T(8,128)} %param.32) | copy-start | bytes 12582916
  4.4 1.8 copy-start.1
  4.4 1.9 copy-start.2
  4.7 2.4 %copy-start.5 = (f32[4,128]{1,0:T(4,128)S(1)}, f32[4,128]{1,0:T(4,128)}, u32[]{:S(2)}) copy-start(f32[4,128]{1,0:T(4,128)} %param.26) | copy-start | bytes 6148
  4.7 3.2 %copy-start.6 = (f32[512]{0:T(512)S(1)}, f32[512]{0:T(512)}, u32[]{:S(2)}) copy-start(f32[512]{0:T(512)} %param.28) | copy-start | bytes 6148
  4.7 3.9 %copy-start.7 = (f32[256]{0:T(256)S(1)}, f32[256]{0:T(256)}, u32[]{:S(2)}) copy-start(f32[256]{0:T(256)} %param.22) | copy-start | bytes 3076
  4.8 3.9 %copy-start.8 = (f32[256]{0:T(256)S(1)}, f32[256]{0:T(256)}, u32[]{:S(2)}) copy-start(f32[256]{0:T(256)} %param.20) | copy-start | bytes 3076
  5.1 2.9 %copy-start.3 = (f32[256,512]{1,0:T(8,128)S(1)}, f32[256,512]{1,0:T(8,128)}, u32[]{:S(2)}) copy-start(f32[256,512]{1,0:T(8,128)} %param.27) | copy-start | bytes 1572868
where the time goes:
time: 190 us
  Pallas kernels  179 us (94%)
  local copies, waits for them, and re-layouts  7.47 us (4%)
  other arithmetic  3.59 us (2%)
    pallas_call x1, Pallas kernels, fused_body(): pl.pallas_call(fused_kernel, out_shape=jax.ShapeDtypeStruct((rows, width)...  179 us

commit v1 on v0

v1 whole, which is shorter than its diff:
```python
import jax
import jax.numpy as jnp
from jax import lax
from jax.experimental import pallas as pl
from jax.experimental.pallas import tpu as pltpu
from jax.sharding import PartitionSpec as P

GDIM = 64
BLOCK = 128


epsilon = 1e-06


def rms_rows(rows, gain):
    floats = rows.astype(jnp.float32)
    scaled = floats * lax.rsqrt(jnp.mean(floats * floats, axis=-1, keepdims=True) + epsilon)
    return (scaled * gain).astype(jnp.bfloat16)


def body(
    tokens,
    mixer_gain,
    direct_weight,
    direct_scale,
    value_weight,
    value_scale,
    value_gain,
    value_shift,
    spatial_weight,
    spatial_bias,
    merge_weight,
    merge_scale,
    channel_gain,
    expand_weight,
    expand_scale,
    reduce_weight,
    reduce_scale,
):
    direct_half = direct_weight.astype(jnp.bfloat16)
    value_half = value_weight.astype(jnp.bfloat16)
    merge_half = merge_weight.astype(jnp.bfloat16)
    expand_half = expand_weight.astype(jnp.bfloat16)
    reduce_half = reduce_weight.astype(jnp.bfloat16)
    full_expand, full_reduce, reduce_full_scale = (
        lax.all_gather(expand_half, "fs", axis=0, tiled=True),
        lax.all_gather(reduce_half, "fs", axis=1, tiled=True),
        lax.all_gather(reduce_scale.astype(jnp.bfloat16), "fs", axis=0, tiled=True).astype(
            reduce_scale.dtype
        ),
    )
    normed = rms_rows(tokens, mixer_gain)
    whole = lax.all_gather(normed, "tp", axis=0, tiled=True)
    seq_rows = whole.shape[0]
    local_width = direct_weight.shape[1]
    direct_pre = jnp.dot(
        whole,
        lax.all_gather(direct_half, "fs", axis=0, tiled=True),
        preferred_element_type=jnp.float32,
    )
    value_pre = jnp.dot(
        whole,
        lax.all_gather(value_half, "fs", axis=0, tiled=True),
        preferred_element_type=jnp.float32,
    )
    full_merge, merge_full_scale = (
        lax.all_gather(merge_half, "fs", axis=1, tiled=True),
        lax.all_gather(merge_scale.astype(jnp.bfloat16), "fs", axis=0, tiled=True).astype(
            merge_scale.dtype
        ),
    )
    direct = jax.nn.gelu(direct_pre * direct_scale)
    value = jax.nn.gelu(value_pre * value_scale)
    total, squares = lax.psum((jnp.sum(value, axis=1), jnp.sum(value * value, axis=1)), "tp")
    branch_width = local_width * lax.axis_size("tp")
    mean = (total / branch_width)[:, None]
    var = (squares / branch_width)[:, None] - mean * mean
    gated_value = ((value - mean) * lax.rsqrt(var + epsilon) * value_gain + value_shift).astype(
        jnp.bfloat16
    )
    local_groups = spatial_weight.shape[0]
    blocks = gated_value.reshape(seq_rows // BLOCK, BLOCK, local_groups, GDIM)
    mixed = jnp.einsum("gpq,nqgc->npgc", spatial_weight, blocks, preferred_element_type=jnp.float32)
    mixed = mixed + jnp.transpose(spatial_bias)[None, :, :, None]
    gated = (direct * mixed.reshape(seq_rows, local_width)).astype(jnp.bfloat16)
    rows = gated
    mix = lax.psum_scatter(
        (jnp.dot(rows, full_merge, preferred_element_type=jnp.float32) * merge_full_scale).astype(
            jnp.bfloat16
        ),
        "tp",
        scatter_dimension=0,
        tiled=True,
    ).astype(jnp.float32)
    middle = (tokens.astype(jnp.float32) + mix).astype(jnp.bfloat16)
    normed_mid = rms_rows(middle, channel_gain)
    whole_mid = lax.all_gather(normed_mid, "tp", axis=0, tiled=True)
    upper = jnp.dot(whole_mid, full_expand, preferred_element_type=jnp.float32)
    hidden = jnp.square(jax.nn.relu(upper * expand_scale)).astype(jnp.bfloat16)
    rows = hidden
    lower = lax.psum_scatter(
        (jnp.dot(rows, full_reduce, preferred_element_type=jnp.float32) * reduce_full_scale).astype(
            jnp.bfloat16
        ),
        "tp",
        scatter_dimension=0,
        tiled=True,
    ).astype(jnp.float32)
    return (middle.astype(jnp.float32) + lower).astype(jnp.bfloat16)


MESH = pl.DeviceIdType.MESH


def fused_kernel(
    tok_ref, mgain_ref, dscale_ref, vscale_ref, vgain_ref, vshift_ref, sw_ref, sbias_ref,
    mscale_ref, cgain_ref, exscale_ref, rscale_ref,
    dw_ref, vw_ref, mw_ref, ew_ref, rw_ref,
    out_ref,
    dv_f32, mg_f32, ex_f32, rd_f32,
    dv_all, mg_all, ex_all, ex_out, rd_all, rd_out,
    xg, act, stat, gated, p1, r1, s1, x1, mid,
    nm, hid, p2, r2, f1, a1, f2, a2, f3, a3,
    load_sem, wsend, wrecv, xsend, xrecv, csend, crecv, gsend, grecv, tsend, trecv, msend, mrecv,
    nsend, nrecv, fsend, frecv,
):
    rows, width = tok_ref.shape
    piece, local = dw_ref.shape
    unit = hid.shape[2]
    half = rows // 2
    thin = piece // 2
    r = lax.axis_index("rep")
    f = lax.axis_index("fs")
    t = lax.axis_index("tp")
    y, c = t // 2, t % 2
    z = f % 2
    mate = f + 1 - 2 * z
    peers = (mate, (f + 2) % 4, (mate + 2) % 4)
    sib = {"tp": y * 2 + (1 - c)}
    ynb = {"tp": (1 - y) * 2 + c}
    xnb = {"rep": 1 - r}
    znb = {"fs": mate}

    barrier = pltpu.get_barrier_semaphore()
    for dev in (sib, ynb, xnb) + tuple({"fs": peer} for peer in peers):
        pl.semaphore_signal(barrier, inc=1, device_id=dev, device_id_type=MESH)

    def span(start, size):
        return pl.ds(pl.multiple_of(start, size), size)

    loads = [
        pltpu.make_async_copy(source, target, load_sem.at[i])
        for i, (source, target) in enumerate(
            (
                (dw_ref, dv_f32.at[0]),
                (vw_ref, dv_f32.at[1]),
                (mw_ref, mg_f32),
                (ew_ref.at[:, span((r * 2 + z) * unit, unit)], ex_f32.at[0]),
                (ew_ref.at[:, span((r * 2 + 1 - z) * unit, unit)], ex_f32.at[1]),
                (rw_ref.at[span((r * 2 + z) * unit, unit)], rd_f32.at[0]),
                (rw_ref.at[span((r * 2 + 1 - z) * unit, unit)], rd_f32.at[1]),
            )
        )
    ]
    for load in loads:
        load.start()

    def rcopy(src, dst, ssem, rsem, dev):
        return pltpu.make_async_remote_copy(
            src_ref=src, dst_ref=dst, send_sem=ssem, recv_sem=rsem,
            device_id=dev, device_id_type=MESH,
        )

    def item(i, slot, q):
        if i < 2:
            return dv_all.at[slot, span(q * 2 * rows + i * rows, rows)]
        return mg_all.at[slot, span(q * rows, rows)]

    def origin(way, d):
        return lax.rem(f + (4 - d if way == 0 else d), 4)

    def comes(way, d):
        return f >= d if way == 0 else f + d <= 3

    def goes(way):
        return f < 3 if way == 0 else f > 0

    def inward(way):
        return f < 2 if way == 0 else f >= 2

    def hop(i, way, d):
        ref = item(i, origin(way, d), r)
        to = lax.rem(f + (1 if way == 0 else 3), 4)
        return rcopy(ref, ref, wsend.at[i, way, d], wrecv.at[i, way, d], {"fs": to})

    def over(i, way, d):
        ref = item(i, origin(way, d), r)
        return rcopy(ref, ref, xsend.at[i, way, d - 1], xrecv.at[i, way, d - 1], xnb)

    def relay(i, d):
        for way in range(2):

            @pl.when(comes(way, d))
            def _(way=way):
                hop(i, way, d - 1).wait_recv()
                over(i, way, d).start()

            if d < 3:

                @pl.when(jnp.logical_and(comes(way, d), goes(way)))
                def _(way=way):
                    hop(i, way, d).start()

    def over_wait(i, d):
        for way in range(2):

            @pl.when(comes(way, d))
            def _(way=way):
                over(i, way, d).wait_recv()

    def ex_slot(slot):
        return ex_all.at[span(slot * piece, piece)]

    def chunk(i, j):
        if i == 0:
            src, dst = (ex_slot(f) if j == 1 else ex_out), ex_slot(f)
        else:
            src = rd_all.at[f, i - 1] if j == 1 else rd_out.at[i - 1]
            dst = rd_all.at[f, i - 1]
        return rcopy(src, dst, csend.at[i, j], crecv.at[i, j], {"fs": peers[j]})

    def norm(x, gain):
        return (
            x * lax.rsqrt(jnp.mean(x * x, axis=-1, keepdims=True) + epsilon) * gain
        ).astype(jnp.bfloat16)

    def block(n, size=1):
        return pl.ds(pl.multiple_of(n * rows, rows), size * rows)

    def columns(slot):
        return span(slot * piece, piece)

    for i in range(2):
        loads[i].wait()
        dv_all[f, :, i * local : (i + 1) * local] = dv_f32[i].astype(jnp.bfloat16)
    mine = xg.at[block(c * 2 + y)]
    mine[...] = norm(tok_ref[...].astype(jnp.float32), mgain_ref[...])
    far = xg.at[block(c * 2 + 1 - y)]
    gather = (
        rcopy(mine, mine, gsend.at[0], grecv.at[0], sib),
        rcopy(mine, mine, gsend.at[1], grecv.at[1], ynb),
        rcopy(far, far, gsend.at[2], grecv.at[2], sib),
    )
    pl.semaphore_wait(barrier, 6)
    for i in range(2):
        for way in range(2):

            @pl.when(goes(way))
            def _(i=i, way=way):
                hop(i, way, 0).start()

    gather[1].start()
    gather[0].start()
    loads[2].wait()
    mg_all[f] = (mg_f32[...] * mscale_ref[...]).astype(jnp.bfloat16)
    loads[3].wait()
    ex_all[columns(f)] = ex_f32[0].astype(jnp.bfloat16)
    loads[4].wait()
    ex_out[...] = ex_f32[1].astype(jnp.bfloat16)
    relay(0, 1)
    relay(1, 1)
    for way in range(2):

        @pl.when(inward(way))
        def _(way=way):
            hop(2, way, 0).start()

    relay(0, 2)
    relay(1, 2)
    for way in range(2):

        @pl.when(jnp.logical_and(jnp.logical_not(inward(way)), goes(way)))
        def _(way=way):
            hop(2, way, 0).start()

    gather[1].wait_recv()
    gather[2].start()
    relay(2, 1)
    chunk(0, 1).start()
    inner = jnp.logical_or(f == 1, f == 2)

    @pl.when(inner)
    def _():
        chunk(0, 2).start()

    loads[5].wait()
    rd_all[f, 0] = (rd_f32[0, :, :thin] * rscale_ref[:, :thin]).astype(jnp.bfloat16)
    rd_all[f, 1] = (rd_f32[0, :, thin:] * rscale_ref[:, thin:]).astype(jnp.bfloat16)
    loads[6].wait()
    rd_out[0] = (rd_f32[1, :, :thin] * rscale_ref[:, :thin]).astype(jnp.bfloat16)
    rd_out[1] = (rd_f32[1, :, thin:] * rscale_ref[:, thin:]).astype(jnp.bfloat16)

    def project(slot):
        return jnp.dot(xg[:, columns(slot)], dv_all[slot], preferred_element_type=jnp.float32)

    gather[0].wait_recv()
    gather[2].wait_recv()
    act[...] = project(f)
    relay(0, 3)
    relay(1, 3)
    relay(2, 2)

    def project_more(d):
        for i in range(2):
            over_wait(i, d)
        for way in range(2):

            @pl.when(comes(way, d))
            def _(way=way):
                act[...] += project(origin(way, d))

    project_more(1)
    project_more(2)
    project_more(3)
    relay(2, 3)
    dvscale = jnp.concatenate([dscale_ref[...], vscale_ref[...]], axis=1)
    act[...] = jax.nn.gelu(act[...] * dvscale)

    lane = lax.broadcasted_iota(jnp.int32, (rows, rows), 1)
    for n in range(4):
        value = act[n * rows : (n + 1) * rows, local:]
        total = jnp.sum(value, axis=1, keepdims=True)
        squares = jnp.sum(value * value, axis=1, keepdims=True)
        table = jnp.where(lane == 0, total, jnp.where(lane == 1, squares, 0.0))
        stat[t, n] = jnp.transpose(table)[:8]
    stats = [
        rcopy(stat.at[t], stat.at[t], tsend.at[0], trecv.at[0], sib),
        rcopy(stat.at[t], stat.at[t], tsend.at[1], trecv.at[1], ynb),
        rcopy(
            stat.at[(1 - y) * 2 + c], stat.at[(1 - y) * 2 + c], tsend.at[2], trecv.at[2], sib
        ),
    ]
    stats[1].start()
    stats[0].start()
    groups = sbias_ref.shape[0]
    down = lax.broadcasted_iota(jnp.int32, (rows, rows), 0)
    bias = jnp.zeros((rows, rows), jnp.float32)
    for n in range(groups):
        bias = jnp.where(down == n, sbias_ref[n : n + 1, :], bias)
    bias = jnp.transpose(bias)
    stats[1].wait_recv()
    stats[2].start()
    stats[0].wait_recv()
    stats[2].wait_recv()
    inverse = 1.0 / (local * 4)
    group_lane = lax.broadcasted_iota(jnp.int32, (rows, 128), 1) // GDIM
    for n in range(4):
        here = slice(n * rows, (n + 1) * rows)
        summed = stat[0, n] + stat[1, n] + stat[2, n] + stat[3, n]
        table = jnp.transpose(jnp.concatenate([summed] * (rows // 8), axis=0))
        mean = table[:, 0:1] * inverse
        var = table[:, 1:2] * inverse - mean * mean
        gv = (
            (act[here, local:] - mean) * lax.rsqrt(var + epsilon) * vgain_ref[...]
            + vshift_ref[...]
        ).astype(jnp.bfloat16)
        per = 128 // GDIM
        for j in range(local // 128):
            at = slice(j * 128, (j + 1) * 128)
            mixed = jnp.dot(sw_ref[j * per], gv[:, at], preferred_element_type=jnp.float32)
            mixed = mixed + bias[:, j * per : j * per + 1]
            for k in range(1, per):
                n_group = j * per + k
                other = jnp.dot(sw_ref[n_group], gv[:, at], preferred_element_type=jnp.float32)
                other = other + bias[:, n_group : n_group + 1]
                mixed = jnp.where(group_lane == k, other, mixed)
            gated[here, at] = (act[here, at] * mixed).astype(jnp.bfloat16)

    base = f - z
    order = (base, base + 1, 2 - base, 3 - base)

    def merge_pair(k):
        return rcopy(
            p1.at[k, block((1 - c) * 2, 2)], r1.at[k], msend.at[k, 0], mrecv.at[k, 0], sib
        )

    def merge_far(k):
        return rcopy(s1.at[k], x1.at[k], msend.at[k, 1], mrecv.at[k, 1], ynb)

    def merge_send(k):
        merge_pair(k).wait_recv()
        s1[k] = (
            p1[k, block(c * 2 + 1 - y)].astype(jnp.float32)
            + r1[k, block(1 - y)].astype(jnp.float32)
        ).astype(jnp.bfloat16)
        merge_far(k).start()

    for k, slot in enumerate(order):
        if k == 0:
            for d in range(1, 4):
                over_wait(2, d)
        p1[k] = jnp.dot(gated[...], mg_all[slot], preferred_element_type=jnp.float32).astype(
            jnp.bfloat16
        )
        merge_pair(k).start()
        if k > 0:
            merge_send(k - 1)
    merge_send(3)
    for k, slot in enumerate(order):
        merge_far(k).wait_recv()
        mid[:, columns(slot)] = (
            tok_ref[:, columns(slot)].astype(jnp.float32)
            + p1[k, block(c * 2 + y)].astype(jnp.float32)
            + r1[k, block(y)].astype(jnp.float32)
            + x1[k].astype(jnp.float32)
        ).astype(jnp.bfloat16)

    def group(zz, rr, yy):
        return zz * 4 + rr * 2 + yy

    def place(zz, rr, yy):
        return nm.at[group(zz, rr, yy), c]

    mine = place(z, r, y)
    mine[...] = norm(mid[...].astype(jnp.float32), cgain_ref[...])
    over_fs = rcopy(mine, mine, nsend.at[20], nrecv.at[20], znb)

    def spreading(b, zz):
        here, from_x = place(zz, r, y), place(zz, 1 - r, y)
        from_y, from_xy = place(zz, r, 1 - y), place(zz, 1 - r, 1 - y)

        def low(ref):
            return ref.at[pl.ds(0, half)]

        def high(ref):
            return ref.at[pl.ds(half, half)]

        routes = (
            (low(here), xnb), (high(here), xnb), (high(here), ynb), (low(here), ynb), (here, sib),
            (low(from_x), ynb), (high(from_y), xnb),
            (from_x, sib), (from_y, sib), (from_xy, sib),
        )
        return tuple(
            rcopy(ref, ref, nsend.at[10 * b + k], nrecv.at[10 * b + k], dev)
            for k, (ref, dev) in enumerate(routes)
        )

    near, away = spreading(0, z), spreading(1, 1 - z)

    def first(spread):
        for k in (0, 2, 1, 3, 4):
            spread[k].start()

    def second(spread):
        spread[0].wait_recv()
        spread[5].start()
        spread[2].wait_recv()
        spread[6].start()

    def third(spread):
        spread[1].wait_recv()
        spread[7].start()
        spread[3].wait_recv()
        spread[8].start()

    def fourth(spread):
        spread[5].wait_recv()
        spread[6].wait_recv()
        spread[9].start()

    def gathered(spread):
        for k in (4, 7, 8, 9):
            spread[k].wait_recv()

    over_fs.start()
    first(near)

    @pl.when(jnp.logical_not(inner))
    def _():
        chunk(0, 2).start()

    chunk(0, 0).start()
    for i in range(1, 3):
        chunk(i, 0).start()
    for i in range(1, 3):
        for j in range(1, 3):
            chunk(i, j).start()
    second(near)
    third(near)
    over_fs.wait_recv()
    first(away)
    fourth(near)
    second(away)
    third(away)

    tall = 2 * rows
    exscale = exscale_ref[:, span((r * 2 + z) * unit, unit)]

    def expand(zz):
        def step(i, _):
            g = zz * 4 + i
            upper = jnp.dot(
                nm[g].reshape(tall, width), ex_all[...], preferred_element_type=jnp.float32
            ) * exscale
            hid[g] = jnp.square(jax.nn.relu(upper)).astype(jnp.bfloat16)

        lax.fori_loop(0, 4, step, None)

    steps = ((0, 0), (1, 0), (0, 1), (1, 1), (2, 0), (3, 0), (2, 1), (3, 1))
    near_half, far_half = 0, 1
    units = tuple((k, h) for h in range(2) for k in range(4)) + tuple(
        (k + p, h) for k in (4, 6) for h in range(2) for p in range(2)
    )

    def plane(h):
        return z if h == near_half else 1 - z

    def arrived(side, j):
        rcopy(
            rd_out.at[side], rd_all.at[f, side], csend.at[1 + side, j], crecv.at[1 + side, j], znb
        ).wait_recv()

    def reduce(u):
        k, h = units[u]
        from_slot, side = steps[k]
        slot = order[from_slot]
        if h == near_half:
            if from_slot == 0:
                arrived(side, 0)
            elif from_slot > 1:
                arrived(side, 1 + (from_slot + z) % 2)
        zz = plane(h)

        def step(i, _):
            g = zz * 4 + i * 2
            p2[k, pl.ds(g, 2)] = (
                jnp.dot(
                    hid[pl.ds(g, 2)].reshape(2 * tall, unit), rd_all[slot, side],
                    preferred_element_type=jnp.float32,
                )
                .astype(jnp.bfloat16)
                .reshape(2, 2, rows, thin)
            )

        lax.fori_loop(0, 2, step, None)
        pair(u).start()

    def pair(u):
        k, h = units[u]
        at = pl.ds(plane(h) * 4, 4)
        return rcopy(p2.at[k, at, 1 - c], r2.at[k, at], fsend.at[0, u], frecv.at[0, u], sib)

    def summed_pair(k, g):
        return p2[k, g, c].astype(jnp.float32) + r2[k, g].astype(jnp.float32)

    def hop_one(u):
        return rcopy(
            f1.at[u], a1.at[u], fsend.at[1, u], frecv.at[1, u], (ynb, xnb)[units[u][0] % 2]
        )

    def hop_two(u):
        return rcopy(
            f2.at[u], a2.at[u], fsend.at[2, u], frecv.at[2, u], (xnb, ynb)[units[u][0] % 2]
        )

    def hop_three(k):
        return rcopy(f3.at[k], a3.at[k], fsend.at[3, k], frecv.at[3, k], znb)

    def send_one(u):
        k, h = units[u]
        zz = plane(h)
        pair(u).wait_recv()
        for n in range(2):
            g = group(zz, n, 1 - y) if k % 2 == 0 else group(zz, 1 - r, n)
            f1[u, n] = summed_pair(k, g).astype(jnp.bfloat16)
        hop_one(u).start()

    def send_two(u):
        k, h = units[u]
        zz = plane(h)
        hop_one(u).wait_recv()
        g, n = (group(zz, 1 - r, y), 1 - r) if k % 2 == 0 else (group(zz, r, 1 - y), 1 - y)
        f2[u] = (summed_pair(k, g) + a1[u, n].astype(jnp.float32)).astype(jnp.bfloat16)
        hop_two(u).start()

    def own_sum(u):
        k, h = units[u]
        n = r if k % 2 == 0 else y
        hop_two(u).wait_recv()
        return (
            summed_pair(k, group(plane(h), r, y))
            + a1[u, n].astype(jnp.float32)
            + a2[u].astype(jnp.float32)
        )

    def send_three(u):
        k, h = units[u]
        if h == far_half:
            f3[k] = own_sum(u).astype(jnp.bfloat16)
            hop_three(k).start()

    for j in range(3):
        chunk(0, j).wait_recv()
    gathered(near)
    expand(z)
    done = set()

    def once(action, u):
        if 0 <= u < len(units) and (action, u) not in done:
            done.add((action, u))
            action(u)

    for u in range(len(units) + 5):
        if u == 4:
            once(send_one, 3)
            fourth(away)
            gathered(away)
            expand(1 - z)
            once(send_two, 0)
        if u == 8:
            once(send_one, 7)
        once(reduce, u)
        once(send_one, u - 1)
        if u != 3:
            once(send_two, u - 3)
        once(send_three, u - 5)
    for k, (from_slot, side) in enumerate(steps):
        at = span(order[from_slot] * piece + side * thin, thin)
        near_sum = own_sum(units.index((k, near_half)))
        hop_three(k).wait_recv()
        out_ref[:, at] = (
            mid[:, at].astype(jnp.float32) + near_sum + a3[k].astype(jnp.float32)
        ).astype(jnp.bfloat16)

    for i in range(3):
        for way in range(2):
            for d in range(3):

                @pl.when(jnp.logical_and(comes(way, d), goes(way)))
                def _(i=i, way=way, d=d):
                    hop(i, way, d).wait_send()

                @pl.when(comes(way, d + 1))
                def _(i=i, way=way, d=d):
                    over(i, way, d + 1).wait_send()

        for j in range(3):
            chunk(i, j).wait_send()
    for copy in gather + tuple(stats) + near + away + (over_fs,):
        copy.wait_send()
    for k in range(4):
        merge_pair(k).wait_send()
        merge_far(k).wait_send()
    for u in range(len(units)):
        pair(u).wait_send()
        hop_one(u).wait_send()
        hop_two(u).wait_send()
    for k in range(len(steps)):
        hop_three(k).wait_send()


def fused_body(
    tokens,
    mixer_gain,
    direct_weight,
    direct_scale,
    value_weight,
    value_scale,
    value_gain,
    value_shift,
    spatial_weight,
    spatial_bias,
    merge_weight,
    merge_scale,
    channel_gain,
    expand_weight,
    expand_scale,
    reduce_weight,
    reduce_scale,
):
    bf = jnp.bfloat16
    rows, width = tokens.shape
    piece, local = direct_weight.shape
    unit = expand_weight.shape[1] // 4
    thin = piece // 2
    seq = 4 * rows
    vm = pltpu.VMEM
    dma = pltpu.SemaphoreType.DMA
    f32 = jnp.float32
    small = (
        tokens, mixer_gain[None], direct_scale[None], value_scale[None], value_gain[None],
        value_shift[None], spatial_weight, spatial_bias, merge_scale[None], channel_gain[None],
        expand_scale[None], reduce_scale[None],
    )
    large = (direct_weight, value_weight, merge_weight, expand_weight, reduce_weight)
    return pl.pallas_call(
        fused_kernel,
        out_shape=jax.ShapeDtypeStruct((rows, width), bf),
        in_specs=[pl.BlockSpec(memory_space=pltpu.VMEM)] * len(small)
        + [pl.BlockSpec(memory_space=pl.ANY)] * len(large),
        out_specs=pl.BlockSpec(memory_space=pltpu.VMEM),
        scratch_shapes=[
            vm((2, piece, local), f32),
            vm((local, piece), f32),
            vm((2, piece, unit), f32),
            vm((2, unit, piece), f32),
            vm((4, piece, 2 * local), bf),
            vm((4, local, piece), bf),
            vm((4 * piece, unit), bf),
            vm((piece, unit), bf),
            vm((4, 2, unit, thin), bf),
            vm((2, unit, thin), bf),
            vm((seq, width), bf),
            vm((seq, 2 * local), f32),
            vm((4, 4, 8, rows), f32),
            vm((seq, local), bf),
            vm((4, seq, piece), bf),
            vm((4, 2 * rows, piece), bf),
            vm((4, rows, piece), bf),
            vm((4, rows, piece), bf),
            vm((rows, width), bf),
            vm((8, 2, rows, width), bf),
            vm((8, 2 * rows, unit), bf),
            vm((8, 8, 2, rows, thin), bf),
            vm((8, 8, rows, thin), bf),
            vm((16, 2, rows, thin), bf),
            vm((16, 2, rows, thin), bf),
            vm((16, rows, thin), bf),
            vm((16, rows, thin), bf),
            vm((8, rows, thin), bf),
            vm((8, rows, thin), bf),
            dma((7,)),
            dma((3, 2, 3)), dma((3, 2, 3)),
            dma((3, 2, 3)), dma((3, 2, 3)),
            dma((3, 3)), dma((3, 3)),
            dma((3,)), dma((3,)),
            dma((3,)), dma((3,)),
            dma((4, 2)), dma((4, 2)),
            dma((21,)), dma((21,)),
            dma((4, 16)), dma((4, 16)),
        ],
        compiler_params=pltpu.CompilerParams(
            collective_id=0, has_side_effects=True, vmem_limit_bytes=62 * 1024 * 1024
        ),
    )(*small, *large)


def solution(mesh):
    sizes = mesh.shape
    fused = sizes["rep"] == 2 and sizes["fs"] == 4 and sizes["tp"] == 4
    return jax.shard_map(
        fused_body if fused else body,
        mesh=mesh,
        in_specs=(
            P(("rep", "fs", "tp"), None),
            P(),
            P("fs", "tp"),
            P("tp"),
            P("fs", "tp"),
            P("tp"),
            P("tp"),
            P("tp"),
            P("tp", None, None),
            P("tp", None),
            P("tp", "fs"),
            P("fs"),
            P(),
            P("fs", "tp"),
            P("tp"),
            P("tp", "fs"),
            P("fs"),
        ),
        out_specs=P(("rep", "fs", "tp"), None),
        check_vma=False,
    )
```

time: 190 us -> 166 us (0.87)
  Pallas kernels: 179 us -> 164 us
  local copies, waits for them, and re-layouts: 7.47 us -> 1.88 us
  other arithmetic: 3.59 us -> 0 us
    pallas_call x1, Pallas kernels: 179 us -> 164 us  [fused_body(): pl.pallas_call(fused_kernel, out_shape=jax.ShapeDtypeStruct((rows, width)...]
    reshape x3 -> x0, local copies, waits for them, and re-layouts: 2.2 us -> none  [the longest x2 1.45 us: fused_body(): rd = jnp.transpose(rd.reshape(2, unit, 2, piece // 2), (0, 2, 1, 3))]
where the time goes in v1:
time: 166 us
  Pallas kernels  164 us (99%)
  local copies, waits for them, and re-layouts  1.88 us (1%)
    pallas_call x1, Pallas kernels, fused_body(): pl.pallas_call(fused_kernel, out_shape=jax.ShapeDtypeStruct((rows, width)...  164 us

profile of v1, /device:TPU:0, one launch (start us, length us, event | category | flops | bytes accessed | tf_op | source)
XLA Modules:
  0.0 166.3 jit_solution(12272932909751190406)
XLA Ops:
  0.0 164.4 %shard_map.163 = bf16[128,2048]{1,0:T(8,128)(2,1)} custom-call(bf16[128,2048]{1,0:T(8,128)(2,1)} %tok_ref.1, f32[1,2048]{1,0:T(1,128)} %bitcast.9, f32[1,256]{1,0:T(1,128)} %bitcast.14, f32[1,256]{1,0:T(1,128)} %bitcast.15, f32[1,256]{1,0:T(1,128)} %bitcast.16, f32[1,256]{1,0:T(1,128)} %bitcast.17, bf16[4,128,128]{2,1,0:T(8,128)(2,1)} %sw_ref.1, ...), custom_call_target="tpu_custom_call" | custom-call | tf_op jit(solution)/shard_map/pallas_call | solution.py:696
  164.4 1.9 %copy.19 = bf16[128,2048]{1,0:T(8,128)(2,1)} copy(bf16[128,2048]{1,0:T(8,128)(2,1)} %shard_map.163) | data formatting | bytes 1048576

commit v2 on v1

--- a/solution.py
+++ b/solution.py
@@ -118,7 +118,7 @@
     dw_ref, vw_ref, mw_ref, ew_ref, rw_ref,
     out_ref,
     dv_f32, mg_f32, ex_f32, rd_f32,
-    dv_all, mg_all, ex_all, ex_out, rd_all, rd_out,
+    dv_all, mg_all, ex_all, ex_own, rd_all, rd_own,
     xg, act, stat, gated, p1, r1, s1, x1, mid,
     nm, hid, p2, r2, f1, a1, f2, a2, f3, a3,
     load_sem, wsend, wrecv, xsend, xrecv, csend, crecv, gsend, grecv, tsend, trecv, msend, mrecv,
@@ -126,7 +126,9 @@
 ):
     rows, width = tok_ref.shape
     piece, local = dw_ref.shape
-    unit = hid.shape[2]
+    big = hid.shape[2]
+    wide = ex_own.shape[1]
+    small = wide - big
     half = rows // 2
     thin = piece // 2
     r = lax.axis_index("rep")
@@ -155,10 +157,8 @@
                 (dw_ref, dv_f32.at[0]),
                 (vw_ref, dv_f32.at[1]),
                 (mw_ref, mg_f32),
-                (ew_ref.at[:, span((r * 2 + z) * unit, unit)], ex_f32.at[0]),
-                (ew_ref.at[:, span((r * 2 + 1 - z) * unit, unit)], ex_f32.at[1]),
-                (rw_ref.at[span((r * 2 + z) * unit, unit)], rd_f32.at[0]),
-                (rw_ref.at[span((r * 2 + 1 - z) * unit, unit)], rd_f32.at[1]),
+                (ew_ref.at[:, span(r * wide, wide)], ex_f32),
+                (rw_ref.at[span(r * wide, wide)], rd_f32),
             )
         )
     ]
@@ -218,16 +218,43 @@
             def _(way=way):
                 over(i, way, d).wait_recv()
 
-    def ex_slot(slot):
-        return ex_all.at[span(slot * piece, piece)]
-
-    def chunk(i, j):
-        if i == 0:
-            src, dst = (ex_slot(f) if j == 1 else ex_out), ex_slot(f)
-        else:
-            src = rd_all.at[f, i - 1] if j == 1 else rd_out.at[i - 1]
-            dst = rd_all.at[f, i - 1]
-        return rcopy(src, dst, csend.at[i, j], crecv.at[i, j], {"fs": peers[j]})
+    inner = jnp.logical_or(f == 1, f == 2)
+    outer = jnp.logical_not(inner)
+
+    def part(to_inner):
+        return (0, big) if to_inner else (big, small)
+
+    def ex_copy(j, to_inner, h=None):
+        first, size = part(to_inner)
+        start, count = (0, piece) if h is None else (h * thin, thin)
+        n = j + 1 if h is None else h
+        return rcopy(
+            ex_own.at[pl.ds(start, count), pl.ds(first, size)],
+            ex_all.at[pl.ds(pl.multiple_of(f * piece + start, thin), count), pl.ds(0, size)],
+            csend.at[n], crecv.at[n], {"fs": peers[j]},
+        )
+
+    def rd_copy(side, j, to_inner, index=None):
+        first, size = part(to_inner)
+        n = 4 + side * 3 + (j if index is None else index)
+        return rcopy(
+            rd_own.at[side, pl.ds(first, size)], rd_all.at[f, side, pl.ds(0, size)],
+            csend.at[n], crecv.at[n], {"fs": peers[j]},
+        )
+
+    def both(action):
+        @pl.when(inner)
+        def _():
+            action(True)
+
+        @pl.when(outer)
+        def _():
+            action(False)
+
+    def ex_copies(to_inner):
+        return [ex_copy(0, to_inner[0], 0), ex_copy(0, to_inner[0], 1)] + [
+            ex_copy(j, to_inner[j]) for j in range(1, 3)
+        ]
 
     def norm(x, gain):
         return (
@@ -264,9 +291,8 @@
     loads[2].wait()
     mg_all[f] = (mg_f32[...] * mscale_ref[...]).astype(jnp.bfloat16)
     loads[3].wait()
-    ex_all[columns(f)] = ex_f32[0].astype(jnp.bfloat16)
-    loads[4].wait()
-    ex_out[...] = ex_f32[1].astype(jnp.bfloat16)
+    ex_own[...] = ex_f32[...].astype(jnp.bfloat16)
+
     relay(0, 1)
     relay(1, 1)
     for way in range(2):
@@ -275,6 +301,11 @@
         def _(way=way):
             hop(2, way, 0).start()
 
+    @pl.when(outer)
+    def _():
+        for h in range(2):
+            ex_copy(0, True, h).start()
+
     relay(0, 2)
     relay(1, 2)
     for way in range(2):
@@ -285,20 +316,38 @@
 
     gather[1].wait_recv()
     gather[2].start()
-    relay(2, 1)
-    chunk(0, 1).start()
-    inner = jnp.logical_or(f == 1, f == 2)
 
     @pl.when(inner)
     def _():
-        chunk(0, 2).start()
-
-    loads[5].wait()
-    rd_all[f, 0] = (rd_f32[0, :, :thin] * rscale_ref[:, :thin]).astype(jnp.bfloat16)
-    rd_all[f, 1] = (rd_f32[0, :, thin:] * rscale_ref[:, thin:]).astype(jnp.bfloat16)
-    loads[6].wait()
-    rd_out[0] = (rd_f32[1, :, :thin] * rscale_ref[:, :thin]).astype(jnp.bfloat16)
-    rd_out[1] = (rd_f32[1, :, thin:] * rscale_ref[:, thin:]).astype(jnp.bfloat16)
+        relay(2, 1)
+        relay(2, 2)
+        for h in range(2):
+            ex_copy(0, False, h).start()
+
+    @pl.when(outer)
+    def _():
+        relay(0, 3)
+        relay(1, 3)
+
+    loads[4].wait()
+    for side in range(2):
+        cut = slice(side * thin, (side + 1) * thin)
+        rd_own[side] = (rd_f32[:, cut] * rscale_ref[:, cut]).astype(jnp.bfloat16)
+
+    @pl.when(outer)
+    def _():
+        ex_all[:, small:] = jnp.zeros((width, big - small), jnp.bfloat16)
+        for slot in range(4):
+            for side in range(2):
+                rd_all[slot, side, small:] = jnp.zeros((big - small, thin), jnp.bfloat16)
+
+    def place_own(is_inner):
+        first, size = part(is_inner)
+        ex_all[columns(f), :size] = ex_own[:, first : first + size]
+        for side in range(2):
+            rd_all[f, side, :size] = rd_own[side, first : first + size]
+
+    both(place_own)
 
     def project(slot):
         return jnp.dot(xg[:, columns(slot)], dv_all[slot], preferred_element_type=jnp.float32)
@@ -306,9 +355,6 @@
     gather[0].wait_recv()
     gather[2].wait_recv()
     act[...] = project(f)
-    relay(0, 3)
-    relay(1, 3)
-    relay(2, 2)
 
     def project_more(d):
         for i in range(2):
@@ -322,7 +368,19 @@
     project_more(1)
     project_more(2)
     project_more(3)
-    relay(2, 3)
+
+    @pl.when(outer)
+    def _():
+        ex_copy(1, True).start()
+        ex_copy(2, False).start()
+        relay(2, 1)
+        relay(2, 2)
+
+    @pl.when(inner)
+    def _():
+        ex_copy(2, True).start()
+        ex_copy(1, False).start()
+
     dvscale = jnp.concatenate([dscale_ref[...], vscale_ref[...]], axis=1)
     act[...] = jax.nn.gelu(act[...] * dvscale)
 
@@ -352,6 +410,11 @@
     stats[2].start()
     stats[0].wait_recv()
     stats[2].wait_recv()
+
+    @pl.when(outer)
+    def _():
+        relay(2, 3)
+
     inverse = 1.0 / (local * 4)
     group_lane = lax.broadcasted_iota(jnp.int32, (rows, 128), 1) // GDIM
     for n in range(4):
@@ -376,8 +439,10 @@
                 mixed = jnp.where(group_lane == k, other, mixed)
             gated[here, at] = (act[here, at] * mixed).astype(jnp.bfloat16)
 
-    base = f - z
-    order = (base, base + 1, 2 - base, 3 - base)
+    closer, farther = jnp.where(inner, 2, 1), jnp.where(inner, 1, 2)
+    second_slot = jnp.where(inner, peers[2], peers[1])
+    last_slot = jnp.where(inner, peers[1], peers[2])
+    merge_order = (f, mate, second_slot, last_slot)
 
     def merge_pair(k):
         return rcopy(
@@ -395,10 +460,22 @@
         ).astype(jnp.bfloat16)
         merge_far(k).start()
 
-    for k, slot in enumerate(order):
-        if k == 0:
-            for d in range(1, 4):
-                over_wait(2, d)
+    for k, slot in enumerate(merge_order):
+        if k == 1:
+            over_wait(2, 1)
+        if k == 2:
+
+            @pl.when(outer)
+            def _():
+                over_wait(2, 2)
+
+        if k == 3:
+
+            @pl.when(inner)
+            def _():
+                over_wait(2, 2)
+
+            over_wait(2, 3)
         p1[k] = jnp.dot(gated[...], mg_all[slot], preferred_element_type=jnp.float32).astype(
             jnp.bfloat16
         )
@@ -406,7 +483,7 @@
         if k > 0:
             merge_send(k - 1)
     merge_send(3)
-    for k, slot in enumerate(order):
+    for k, slot in enumerate(merge_order):
         merge_far(k).wait_recv()
         mid[:, columns(slot)] = (
             tok_ref[:, columns(slot)].astype(jnp.float32)
@@ -475,67 +552,79 @@
     over_fs.start()
     first(near)
 
-    @pl.when(jnp.logical_not(inner))
+    @pl.when(outer)
     def _():
-        chunk(0, 2).start()
-
-    chunk(0, 0).start()
-    for i in range(1, 3):
-        chunk(i, 0).start()
-    for i in range(1, 3):
-        for j in range(1, 3):
-            chunk(i, j).start()
+        for side in range(2):
+            rd_copy(side, 0, True).start()
+        for side in range(2):
+            rd_copy(side, 2, False).start()
+            rd_copy(side, 1, True).start()
+
+    @pl.when(inner)
+    def _():
+        for side in range(2):
+            rd_copy(side, 0, False).start()
+            rd_copy(side, 2, True).start()
+            rd_copy(side, 1, False).start()
+
     second(near)
     third(near)
     over_fs.wait_recv()
     first(away)
     fourth(near)
-    second(away)
-    third(away)
 
     tall = 2 * rows
-    exscale = exscale_ref[:, span((r * 2 + z) * unit, unit)]
-
-    def expand(zz):
+    start = pl.multiple_of(r * wide, wide)
+    exscale = jnp.where(
+        inner,
+        exscale_ref[:, pl.ds(start, big)],
+        jnp.concatenate(
+            [
+                exscale_ref[:, pl.ds(pl.multiple_of(start + big, 2 * GDIM), small)],
+                jnp.zeros((1, big - small), jnp.float32),
+            ],
+            axis=1,
+        ),
+    )
+
+    def expand(count, group_of):
         def step(i, _):
-            g = zz * 4 + i
+            g = group_of(i)
             upper = jnp.dot(
                 nm[g].reshape(tall, width), ex_all[...], preferred_element_type=jnp.float32
             ) * exscale
             hid[g] = jnp.square(jax.nn.relu(upper)).astype(jnp.bfloat16)
 
-        lax.fori_loop(0, 4, step, None)
-
-    steps = ((0, 0), (1, 0), (0, 1), (1, 1), (2, 0), (3, 0), (2, 1), (3, 1))
+        lax.fori_loop(0, count, step, None)
+
+    def pick(if_inner, if_outer):
+        return jnp.where(inner, if_inner, if_outer)
+
+    slots = (f, f, mate, mate, last_slot, last_slot, second_slot, second_slot)
+    sides = (0, 1) * 4
+    came = (None, None, 0, 0) + (pick(1, 2),) * 2 + (pick(2, 1),) * 2
     near_half, far_half = 0, 1
-    units = tuple((k, h) for h in range(2) for k in range(4)) + tuple(
-        (k + p, h) for k in (4, 6) for h in range(2) for p in range(2)
-    )
+    units = ((0, 0), (1, 0), (2, 0), (0, 1), (1, 1), (2, 1))
+    units += tuple((k, h) for k in range(3, 8) for h in range(2))
 
     def plane(h):
         return z if h == near_half else 1 - z
 
     def arrived(side, j):
-        rcopy(
-            rd_out.at[side], rd_all.at[f, side], csend.at[1 + side, j], crecv.at[1 + side, j], znb
-        ).wait_recv()
+        both(lambda is_inner: rd_copy(side, 0, is_inner, j).wait_recv())
 
     def reduce(u):
         k, h = units[u]
-        from_slot, side = steps[k]
-        slot = order[from_slot]
-        if h == near_half:
-            if from_slot == 0:
-                arrived(side, 0)
-            elif from_slot > 1:
-                arrived(side, 1 + (from_slot + z) % 2)
+        slot, side = slots[k], sides[k]
+        if h == near_half and k > 1:
+            arrived(side, came[k])
         zz = plane(h)
 
         def step(i, _):
             g = zz * 4 + i * 2
             p2[k, pl.ds(g, 2)] = (
                 jnp.dot(
-                    hid[pl.ds(g, 2)].reshape(2 * tall, unit), rd_all[slot, side],
+                    hid[pl.ds(g, 2)].reshape(2 * tall, big), rd_all[slot, side],
                     preferred_element_type=jnp.float32,
                 )
                 .astype(jnp.bfloat16)
@@ -555,23 +644,24 @@
 
     def hop_one(u):
         return rcopy(
-            f1.at[u], a1.at[u], fsend.at[1, u], frecv.at[1, u], (ynb, xnb)[units[u][0] % 2]
+            f1.at[u], a1.at[u], fsend.at[1, u], frecv.at[1, u], (ynb, xnb)[u % 2]
         )
 
     def hop_two(u):
         return rcopy(
-            f2.at[u], a2.at[u], fsend.at[2, u], frecv.at[2, u], (xnb, ynb)[units[u][0] % 2]
+            f2.at[u], a2.at[u], fsend.at[2, u], frecv.at[2, u], (xnb, ynb)[u % 2]
         )
 
     def hop_three(k):
-        return rcopy(f3.at[k], a3.at[k], fsend.at[3, k], frecv.at[3, k], znb)
+        q = slots[k] * 2 + sides[k]
+        return rcopy(f3.at[k], a3.at[q], fsend.at[3, k], frecv.at[3, q], znb)
 
     def send_one(u):
         k, h = units[u]
         zz = plane(h)
         pair(u).wait_recv()
         for n in range(2):
-            g = group(zz, n, 1 - y) if k % 2 == 0 else group(zz, 1 - r, n)
+            g = group(zz, n, 1 - y) if u % 2 == 0 else group(zz, 1 - r, n)
             f1[u, n] = summed_pair(k, g).astype(jnp.bfloat16)
         hop_one(u).start()
 
@@ -579,13 +669,13 @@
         k, h = units[u]
         zz = plane(h)
         hop_one(u).wait_recv()
-        g, n = (group(zz, 1 - r, y), 1 - r) if k % 2 == 0 else (group(zz, r, 1 - y), 1 - y)
+        g, n = (group(zz, 1 - r, y), 1 - r) if u % 2 == 0 else (group(zz, r, 1 - y), 1 - y)
         f2[u] = (summed_pair(k, g) + a1[u, n].astype(jnp.float32)).astype(jnp.bfloat16)
         hop_two(u).start()
 
     def own_sum(u):
         k, h = units[u]
-        n = r if k % 2 == 0 else y
+        n = r if u % 2 == 0 else y
         hop_two(u).wait_recv()
         return (
             summed_pair(k, group(plane(h), r, y))
@@ -599,10 +689,10 @@
             f3[k] = own_sum(u).astype(jnp.bfloat16)
             hop_three(k).start()
 
-    for j in range(3):
-        chunk(0, j).wait_recv()
-    gathered(near)
-    expand(z)
+    def ex_arrived(is_inner):
+        for copy in ex_copies((is_inner,) * 3):
+            copy.wait_recv()
+
     done = set()
 
     def once(action, u):
@@ -610,26 +700,41 @@
             done.add((action, u))
             action(u)
 
-    for u in range(len(units) + 5):
-        if u == 4:
-            once(send_one, 3)
-            fourth(away)
-            gathered(away)
-            expand(1 - z)
-            once(send_two, 0)
-        if u == 8:
-            once(send_one, 7)
+    gathered(near)
+    both(ex_arrived)
+    expand(4, lambda i: z * 4 + i)
+    second(away)
+    away[4].wait_recv()
+    expand(1, lambda i: group(1 - z, r, y) + i)
+    once(reduce, 0)
+    once(reduce, 1)
+    third(away)
+    once(send_one, 0)
+    once(send_one, 1)
+    once(reduce, 2)
+    away[7].wait_recv()
+    away[8].wait_recv()
+    expand(2, lambda i: jnp.where(i == 0, group(1 - z, 1 - r, y), group(1 - z, r, 1 - y)))
+    once(send_one, 2)
+    fourth(away)
+    away[9].wait_recv()
+    expand(1, lambda i: group(1 - z, 1 - r, 1 - y) + i)
+    for u in range(3, len(units) + 8):
+        if u == 14:
+            once(send_one, 13)
+            for n in range(10, 14):
+                once(send_two, n)
         once(reduce, u)
         once(send_one, u - 1)
-        if u != 3:
-            once(send_two, u - 3)
-        once(send_three, u - 5)
-    for k, (from_slot, side) in enumerate(steps):
-        at = span(order[from_slot] * piece + side * thin, thin)
+        once(send_two, u - 4)
+        once(send_three, u - 8)
+    for k, (slot, side) in enumerate(zip(slots, sides)):
+        at = span(slot * piece + side * thin, thin)
         near_sum = own_sum(units.index((k, near_half)))
         hop_three(k).wait_recv()
+        q = slot * 2 + side
         out_ref[:, at] = (
-            mid[:, at].astype(jnp.float32) + near_sum + a3[k].astype(jnp.float32)
+            mid[:, at].astype(jnp.float32) + near_sum + a3[q].astype(jnp.float32)
         ).astype(jnp.bfloat16)
 
     for i in range(3):
@@ -644,8 +749,15 @@
                 def _(i=i, way=way, d=d):
                     over(i, way, d + 1).wait_send()
 
-        for j in range(3):
-            chunk(i, j).wait_send()
+    def own_sends(is_inner):
+        to_inner = (not is_inner, not is_inner, is_inner)
+        for copy in ex_copies(to_inner):
+            copy.wait_send()
+        for side in range(2):
+            for j in range(3):
+                rd_copy(side, j, to_inner[j]).wait_send()
+
+    both(own_sends)
     for copy in gather + tuple(stats) + near + away + (over_fs,):
         copy.wait_send()
     for k in range(4):
@@ -655,7 +767,7 @@
         pair(u).wait_send()
         hop_one(u).wait_send()
         hop_two(u).wait_send()
-    for k in range(len(steps)):
+    for k in range(len(slots)):
         hop_three(k).wait_send()
 
 
@@ -681,7 +793,8 @@
     bf = jnp.bfloat16
     rows, width = tokens.shape
     piece, local = direct_weight.shape
-    unit = expand_weight.shape[1] // 4
+    wide = expand_weight.shape[1] // 2
+    big = wide * 5 // 8
     thin = piece // 2
     seq = 4 * rows
     vm = pltpu.VMEM
@@ -702,14 +815,14 @@
         scratch_shapes=[
             vm((2, piece, local), f32),
             vm((local, piece), f32),
-            vm((2, piece, unit), f32),
-            vm((2, unit, piece), f32),
+            vm((piece, wide), f32),
+            vm((wide, piece), f32),
             vm((4, piece, 2 * local), bf),
             vm((4, local, piece), bf),
-            vm((4 * piece, unit), bf),
-            vm((piece, unit), bf),
-            vm((4, 2, unit, thin), bf),
-            vm((2, unit, thin), bf),
+            vm((4 * piece, big), bf),
+            vm((piece, wide), bf),
+            vm((4, 2, big, thin), bf),
+            vm((2, wide, thin), bf),
             vm((seq, width), bf),
             vm((seq, 2 * local), f32),
             vm((4, 4, 8, rows), f32),
@@ -720,7 +833,7 @@
             vm((4, rows, piece), bf),
             vm((rows, width), bf),
             vm((8, 2, rows, width), bf),
-            vm((8, 2 * rows, unit), bf),
+            vm((8, 2 * rows, big), bf),
             vm((8, 8, 2, rows, thin), bf),
             vm((8, 8, rows, thin), bf),
             vm((16, 2, rows, thin), bf),
@@ -729,10 +842,10 @@
             vm((16, rows, thin), bf),
             vm((8, rows, thin), bf),
             vm((8, rows, thin), bf),
-            dma((7,)),
+            dma((5,)),
             dma((3, 2, 3)), dma((3, 2, 3)),
             dma((3, 2, 3)), dma((3, 2, 3)),
-            dma((3, 3)), dma((3, 3)),
+            dma((10,)), dma((10,)),
             dma((3,)), dma((3,)),
             dma((3,)), dma((3,)),
             dma((4, 2)), dma((4, 2)),

time: 166 us -> 140 us (0.84)
  Pallas kernels: 164 us -> 138 us
    pallas_call x1, Pallas kernels: 164 us -> 138 us  [fused_body(): pl.pallas_call(fused_kernel, out_shape=jax.ShapeDtypeStruct((rows, width)...]
where the time goes in v2:
time: 140 us
  Pallas kernels  138 us (99%)
  local copies, waits for them, and re-layouts  1.88 us (1%)
    pallas_call x1, Pallas kernels, fused_body(): pl.pallas_call(fused_kernel, out_shape=jax.ShapeDtypeStruct((rows, width)...  138 us

profile of v2, /device:TPU:0, one launch (start us, length us, event | category | flops | bytes accessed | tf_op | source)
XLA Modules:
  0.0 140.1 jit_solution(254371771187566165)
XLA Ops:
  0.0 138.2 %shard_map.163 = bf16[128,2048]{1,0:T(8,128)(2,1)} custom-call(bf16[128,2048]{1,0:T(8,128)(2,1)} %tok_ref.1, f32[1,2048]{1,0:T(1,128)} %bitcast.9, f32[1,256]{1,0:T(1,128)} %bitcast.14, f32[1,256]{1,0:T(1,128)} %bitcast.15, f32[1,256]{1,0:T(1,128)} %bitcast.16, f32[1,256]{1,0:T(1,128)} %bitcast.17, bf16[4,128,128]{2,1,0:T(8,128)(2,1)} %sw_ref.1, ...), custom_call_target="tpu_custom_call" | custom-call | tf_op jit(solution)/shard_map/pallas_call | solution.py:809
  138.2 1.9 %copy.19 = bf16[128,2048]{1,0:T(8,128)(2,1)} copy(bf16[128,2048]{1,0:T(8,128)(2,1)} %shard_map.163) | data formatting | bytes 1048576

commit v3 on v2

--- a/solution.py
+++ b/solution.py
@@ -113,15 +113,17 @@
 
 
 def fused_kernel(
+    tok_hbm, mgain_hbm, dscale_hbm, vscale_hbm, vgain_hbm, vshift_hbm, sw_hbm, sbias_hbm,
+    mscale_hbm, cgain_hbm, exscale_hbm, rscale_hbm,
+    dw_ref, vw_ref, mw_ref, ew_ref, rw_ref,
+    out_ref,
     tok_ref, mgain_ref, dscale_ref, vscale_ref, vgain_ref, vshift_ref, sw_ref, sbias_ref,
     mscale_ref, cgain_ref, exscale_ref, rscale_ref,
-    dw_ref, vw_ref, mw_ref, ew_ref, rw_ref,
-    out_ref,
     dv_f32, mg_f32, ex_f32, rd_f32,
     dv_all, mg_all, ex_all, ex_own, rd_all, rd_own,
     xg, act, stat, gated, p1, r1, s1, x1, mid,
-    nm, hid, p2, r2, f1, a1, f2, a2, f3, a3,
-    load_sem, wsend, wrecv, xsend, xrecv, csend, crecv, gsend, grecv, tsend, trecv, msend, mrecv,
+    nm, hid, p2, r2, f1, a1, f2, a2, f3, a3, result,
+    load_sem, out_sem, wsend, wrecv, xsend, xrecv, csend, crecv, gsend, grecv, trecv, msend, mrecv,
     nsend, nrecv, fsend, frecv,
 ):
     rows, width = tok_ref.shape
@@ -156,9 +158,21 @@
             (
                 (dw_ref, dv_f32.at[0]),
                 (vw_ref, dv_f32.at[1]),
+                (tok_hbm, tok_ref),
+                (mgain_hbm, mgain_ref),
+                (mscale_hbm, mscale_ref),
                 (mw_ref, mg_f32),
                 (ew_ref.at[:, span(r * wide, wide)], ex_f32),
+                (rscale_hbm, rscale_ref),
                 (rw_ref.at[span(r * wide, wide)], rd_f32),
+                (dscale_hbm, dscale_ref),
+                (vscale_hbm, vscale_ref),
+                (vgain_hbm, vgain_ref),
+                (vshift_hbm, vshift_ref),
+                (sw_hbm, sw_ref),
+                (sbias_hbm, sbias_ref),
+                (cgain_hbm, cgain_ref),
+                (exscale_hbm, exscale_ref),
             )
         )
     ]
@@ -191,18 +205,21 @@
     def hop(i, way, d):
         ref = item(i, origin(way, d), r)
         to = lax.rem(f + (1 if way == 0 else 3), 4)
-        return rcopy(ref, ref, wsend.at[i, way, d], wrecv.at[i, way, d], {"fs": to})
+        return rcopy(
+            ref, ref, wsend.at[min(d, 1)], wrecv.at[i, origin(way, d)], {"fs": to}
+        )
 
     def over(i, way, d):
-        ref = item(i, origin(way, d), r)
-        return rcopy(ref, ref, xsend.at[i, way, d - 1], xrecv.at[i, way, d - 1], xnb)
+        slot = origin(way, d)
+        ref = item(i, slot, r)
+        return rcopy(ref, ref, xsend.at[i // 2], xrecv.at[i, slot], xnb)
 
     def relay(i, d):
         for way in range(2):
 
             @pl.when(comes(way, d))
             def _(way=way):
-                hop(i, way, d - 1).wait_recv()
+                hop(i, way, d).wait_recv()
                 over(i, way, d).start()
 
             if d < 3:
@@ -224,22 +241,27 @@
     def part(to_inner):
         return (0, big) if to_inner else (big, small)
 
-    def ex_copy(j, to_inner, h=None):
+    cuts = ((0, thin // 2), (thin // 2, thin // 2), (thin, thin))
+
+    def ex_copy(j, to_inner, h):
         first, size = part(to_inner)
-        start, count = (0, piece) if h is None else (h * thin, thin)
-        n = j + 1 if h is None else h
+        start, count = cuts[h]
         return rcopy(
             ex_own.at[pl.ds(start, count), pl.ds(first, size)],
-            ex_all.at[pl.ds(pl.multiple_of(f * piece + start, thin), count), pl.ds(0, size)],
-            csend.at[n], crecv.at[n], {"fs": peers[j]},
-        )
+            ex_all.at[span(f * piece + start, count), pl.ds(0, size)],
+            csend.at[int(to_inner)], crecv.at[0], {"fs": peers[j]},
+        )
+
+    def ex_start(j, to_inner, which=(0, 1, 2)):
+        for h in which:
+            ex_copy(j, to_inner, h).start()
 
     def rd_copy(side, j, to_inner, index=None):
         first, size = part(to_inner)
-        n = 4 + side * 3 + (j if index is None else index)
+        n = 1 + side * 3 + (j if index is None else index)
         return rcopy(
             rd_own.at[side, pl.ds(first, size)], rd_all.at[f, side, pl.ds(0, size)],
-            csend.at[n], crecv.at[n], {"fs": peers[j]},
+            csend.at[2 + int(to_inner)], crecv.at[n], {"fs": peers[j]},
         )
 
     def both(action):
@@ -251,11 +273,6 @@
         def _():
             action(False)
 
-    def ex_copies(to_inner):
-        return [ex_copy(0, to_inner[0], 0), ex_copy(0, to_inner[0], 1)] + [
-            ex_copy(j, to_inner[j]) for j in range(1, 3)
-        ]
-
     def norm(x, gain):
         return (
             x * lax.rsqrt(jnp.mean(x * x, axis=-1, keepdims=True) + epsilon) * gain
@@ -270,13 +287,15 @@
     for i in range(2):
         loads[i].wait()
         dv_all[f, :, i * local : (i + 1) * local] = dv_f32[i].astype(jnp.bfloat16)
+    for i in range(2, 4):
+        loads[i].wait()
     mine = xg.at[block(c * 2 + y)]
     mine[...] = norm(tok_ref[...].astype(jnp.float32), mgain_ref[...])
     far = xg.at[block(c * 2 + 1 - y)]
     gather = (
         rcopy(mine, mine, gsend.at[0], grecv.at[0], sib),
-        rcopy(mine, mine, gsend.at[1], grecv.at[1], ynb),
-        rcopy(far, far, gsend.at[2], grecv.at[2], sib),
+        rcopy(mine, mine, gsend.at[0], grecv.at[1], ynb),
+        rcopy(far, far, gsend.at[0], grecv.at[2], sib),
     )
     pl.semaphore_wait(barrier, 6)
     for i in range(2):
@@ -288,9 +307,10 @@
 
     gather[1].start()
     gather[0].start()
-    loads[2].wait()
+    for i in range(4, 6):
+        loads[i].wait()
     mg_all[f] = (mg_f32[...] * mscale_ref[...]).astype(jnp.bfloat16)
-    loads[3].wait()
+    loads[6].wait()
     ex_own[...] = ex_f32[...].astype(jnp.bfloat16)
 
     relay(0, 1)
@@ -303,8 +323,7 @@
 
     @pl.when(outer)
     def _():
-        for h in range(2):
-            ex_copy(0, True, h).start()
+        ex_start(0, True)
 
     relay(0, 2)
     relay(1, 2)
@@ -321,15 +340,15 @@
     def _():
         relay(2, 1)
         relay(2, 2)
-        for h in range(2):
-            ex_copy(0, False, h).start()
+        ex_start(2, True, (0,))
 
     @pl.when(outer)
     def _():
         relay(0, 3)
         relay(1, 3)
 
-    loads[4].wait()
+    for load in loads[7:]:
+        load.wait()
     for side in range(2):
         cut = slice(side * thin, (side + 1) * thin)
         rd_own[side] = (rd_f32[:, cut] * rscale_ref[:, cut]).astype(jnp.bfloat16)
@@ -371,15 +390,9 @@
 
     @pl.when(outer)
     def _():
-        ex_copy(1, True).start()
-        ex_copy(2, False).start()
+        ex_start(1, True, (0, 1))
         relay(2, 1)
         relay(2, 2)
-
-    @pl.when(inner)
-    def _():
-        ex_copy(2, True).start()
-        ex_copy(1, False).start()
 
     dvscale = jnp.concatenate([dscale_ref[...], vscale_ref[...]], axis=1)
     act[...] = jax.nn.gelu(act[...] * dvscale)
@@ -392,10 +405,10 @@
         table = jnp.where(lane == 0, total, jnp.where(lane == 1, squares, 0.0))
         stat[t, n] = jnp.transpose(table)[:8]
     stats = [
-        rcopy(stat.at[t], stat.at[t], tsend.at[0], trecv.at[0], sib),
-        rcopy(stat.at[t], stat.at[t], tsend.at[1], trecv.at[1], ynb),
+        rcopy(stat.at[t], stat.at[t], gsend.at[1], trecv.at[0], sib),
+        rcopy(stat.at[t], stat.at[t], gsend.at[1], trecv.at[1], ynb),
         rcopy(
-            stat.at[(1 - y) * 2 + c], stat.at[(1 - y) * 2 + c], tsend.at[2], trecv.at[2], sib
+            stat.at[(1 - y) * 2 + c], stat.at[(1 - y) * 2 + c], gsend.at[1], trecv.at[2], sib
         ),
     ]
     stats[1].start()
@@ -411,8 +424,14 @@
     stats[0].wait_recv()
     stats[2].wait_recv()
 
+    @pl.when(inner)
+    def _():
+        ex_start(1, False)
+        ex_start(2, True, (1, 2))
+
     @pl.when(outer)
     def _():
+        ex_start(2, False)
         relay(2, 3)
 
     inverse = 1.0 / (local * 4)
@@ -446,11 +465,11 @@
 
     def merge_pair(k):
         return rcopy(
-            p1.at[k, block((1 - c) * 2, 2)], r1.at[k], msend.at[k, 0], mrecv.at[k, 0], sib
+            p1.at[k, block((1 - c) * 2, 2)], r1.at[k], msend.at[0], mrecv.at[k, 0], sib
         )
 
     def merge_far(k):
-        return rcopy(s1.at[k], x1.at[k], msend.at[k, 1], mrecv.at[k, 1], ynb)
+        return rcopy(s1.at[k], x1.at[k], msend.at[1], mrecv.at[k, 1], ynb)
 
     def merge_send(k):
         merge_pair(k).wait_recv()
@@ -500,7 +519,7 @@
 
     mine = place(z, r, y)
     mine[...] = norm(mid[...].astype(jnp.float32), cgain_ref[...])
-    over_fs = rcopy(mine, mine, nsend.at[20], nrecv.at[20], znb)
+    over_fs = rcopy(mine, mine, nsend.at[1], nrecv.at[20], znb)
 
     def spreading(b, zz):
         here, from_x = place(zz, r, y), place(zz, 1 - r, y)
@@ -518,7 +537,7 @@
             (from_x, sib), (from_y, sib), (from_xy, sib),
         )
         return tuple(
-            rcopy(ref, ref, nsend.at[10 * b + k], nrecv.at[10 * b + k], dev)
+            rcopy(ref, ref, nsend.at[0], nrecv.at[10 * b + k], dev)
             for k, (ref, dev) in enumerate(routes)
         )
 
@@ -550,27 +569,39 @@
             spread[k].wait_recv()
 
     over_fs.start()
+
+    @pl.when(outer)
+    def _():
+        ex_start(1, True, (2,))
+
     first(near)
 
-    @pl.when(outer)
-    def _():
-        for side in range(2):
-            rd_copy(side, 0, True).start()
-        for side in range(2):
-            rd_copy(side, 2, False).start()
-            rd_copy(side, 1, True).start()
+    second(near)
 
     @pl.when(inner)
     def _():
-        for side in range(2):
-            rd_copy(side, 0, False).start()
-            rd_copy(side, 2, True).start()
-            rd_copy(side, 1, False).start()
-
-    second(near)
+        ex_start(0, False)
+
     third(near)
     over_fs.wait_recv()
     first(away)
+
+    def rd_start(side, j, to_inner):
+        rd_copy(side, j, to_inner).start()
+
+    @pl.when(inner)
+    def _():
+        for side in range(2):
+            rd_start(side, 0, False)
+        for side in range(2):
+            rd_start(side, 2, True)
+            rd_start(side, 1, False)
+
+    @pl.when(outer)
+    def _():
+        for side in range(2):
+            rd_start(side, 0, True)
+
     fourth(near)
 
     tall = 2 * rows
@@ -600,12 +631,12 @@
     def pick(if_inner, if_outer):
         return jnp.where(inner, if_inner, if_outer)
 
-    slots = (f, f, mate, mate, last_slot, last_slot, second_slot, second_slot)
-    sides = (0, 1) * 4
-    came = (None, None, 0, 0) + (pick(1, 2),) * 2 + (pick(2, 1),) * 2
+    slots = (f, f, mate, mate, second_slot, last_slot, last_slot, second_slot)
+    sides = (0, 1, 0, 1, 0, 0, 1, 1)
+    came = (None, None, 0, 0, pick(2, 1), pick(1, 2), pick(1, 2), pick(2, 1))
     near_half, far_half = 0, 1
-    units = ((0, 0), (1, 0), (2, 0), (0, 1), (1, 1), (2, 1))
-    units += tuple((k, h) for k in range(3, 8) for h in range(2))
+    units = tuple((k, h) for h in range(2) for k in range(4))
+    units += tuple((k, h) for k in range(4, 8) for h in (1, 0))
 
     def plane(h):
         return z if h == near_half else 1 - z
@@ -616,7 +647,7 @@
     def reduce(u):
         k, h = units[u]
         slot, side = slots[k], sides[k]
-        if h == near_half and k > 1:
+        if k > 1 and h == (near_half if k < 4 else far_half):
             arrived(side, came[k])
         zz = plane(h)
 
@@ -637,24 +668,24 @@
     def pair(u):
         k, h = units[u]
         at = pl.ds(plane(h) * 4, 4)
-        return rcopy(p2.at[k, at, 1 - c], r2.at[k, at], fsend.at[0, u], frecv.at[0, u], sib)
+        return rcopy(p2.at[k, at, 1 - c], r2.at[k, at], fsend.at[0], frecv.at[0, u], sib)
 
     def summed_pair(k, g):
         return p2[k, g, c].astype(jnp.float32) + r2[k, g].astype(jnp.float32)
 
     def hop_one(u):
         return rcopy(
-            f1.at[u], a1.at[u], fsend.at[1, u], frecv.at[1, u], (ynb, xnb)[u % 2]
+            f1.at[u], a1.at[u], fsend.at[1], frecv.at[1, u], (ynb, xnb)[u % 2]
         )
 
     def hop_two(u):
         return rcopy(
-            f2.at[u], a2.at[u], fsend.at[2, u], frecv.at[2, u], (xnb, ynb)[u % 2]
+            f2.at[u], a2.at[u], fsend.at[2], frecv.at[2, u], (xnb, ynb)[u % 2]
         )
 
     def hop_three(k):
         q = slots[k] * 2 + sides[k]
-        return rcopy(f3.at[k], a3.at[q], fsend.at[3, k], frecv.at[3, q], znb)
+        return rcopy(f3.at[k], a3.at[q], fsend.at[3], frecv.at[3, q], znb)
 
     def send_one(u):
         k, h = units[u]
@@ -690,8 +721,8 @@
             hop_three(k).start()
 
     def ex_arrived(is_inner):
-        for copy in ex_copies((is_inner,) * 3):
-            copy.wait_recv()
+        ref = ex_all.at[pl.ds(0, 3 * piece), pl.ds(0, part(is_inner)[1])]
+        rcopy(ref, ref, csend.at[0], crecv.at[0], znb).wait_recv()
 
     done = set()
 
@@ -717,58 +748,80 @@
     expand(2, lambda i: jnp.where(i == 0, group(1 - z, 1 - r, y), group(1 - z, r, 1 - y)))
     once(send_one, 2)
     fourth(away)
+
+    @pl.when(outer)
+    def _():
+        for side in range(2):
+            rd_start(side, 2, False)
+            rd_start(side, 1, True)
+
     away[9].wait_recv()
     expand(1, lambda i: group(1 - z, 1 - r, 1 - y) + i)
-    for u in range(3, len(units) + 8):
-        if u == 14:
-            once(send_one, 13)
-            for n in range(10, 14):
-                once(send_two, n)
-        once(reduce, u)
-        once(send_one, u - 1)
-        once(send_two, u - 4)
-        once(send_three, u - 8)
+    turn = (0, 1, 2, 4, 5, 3) + tuple(range(6, len(units)))
+
+    def late(action, n):
+        if n >= 0:
+            once(action, turn[n])
+
+    for n in range(3, len(turn)):
+        if n in (12, 14):
+            late(send_one, n - 1)
+            late(send_two, n - 4)
+            late(send_two, n - 3)
+        late(reduce, n)
+        late(send_one, n - 1)
+        late(send_two, n - 4)
+        late(send_three, n - 8)
+    once(send_one, 15)
+    once(send_two, 12)
+    once(send_three, 8)
+    once(send_two, 13)
+    once(send_three, 10)
+    once(send_two, 14)
+    once(send_three, 12)
+    once(send_two, 15)
+    once(send_three, 14)
+
+    def stored(k):
+        at = span(slots[k] * piece + sides[k] * thin, thin)
+        return pltpu.make_async_copy(result.at[:, at], out_ref.at[:, at], out_sem)
+
     for k, (slot, side) in enumerate(zip(slots, sides)):
         at = span(slot * piece + side * thin, thin)
         near_sum = own_sum(units.index((k, near_half)))
         hop_three(k).wait_recv()
         q = slot * 2 + side
-        out_ref[:, at] = (
+        result[:, at] = (
             mid[:, at].astype(jnp.float32) + near_sum + a3[q].astype(jnp.float32)
         ).astype(jnp.bfloat16)
-
-    for i in range(3):
-        for way in range(2):
-            for d in range(3):
-
-                @pl.when(jnp.logical_and(comes(way, d), goes(way)))
-                def _(i=i, way=way, d=d):
-                    hop(i, way, d).wait_send()
-
-                @pl.when(comes(way, d + 1))
-                def _(i=i, way=way, d=d):
-                    over(i, way, d + 1).wait_send()
-
-    def own_sends(is_inner):
-        to_inner = (not is_inner, not is_inner, is_inner)
-        for copy in ex_copies(to_inner):
-            copy.wait_send()
-        for side in range(2):
-            for j in range(3):
-                rd_copy(side, j, to_inner[j]).wait_send()
-
-    both(own_sends)
-    for copy in gather + tuple(stats) + near + away + (over_fs,):
-        copy.wait_send()
-    for k in range(4):
-        merge_pair(k).wait_send()
-        merge_far(k).wait_send()
-    for u in range(len(units)):
-        pair(u).wait_send()
-        hop_one(u).wait_send()
-        hop_two(u).wait_send()
-    for k in range(len(slots)):
-        hop_three(k).wait_send()
+        stored(k).start()
+
+    def sent(ref, sem):
+        rcopy(ref, ref, sem, crecv.at[0], znb).wait_send()
+
+    def few_sent(is_inner):
+        own = rows * (2 if is_inner else 1)
+        sent(dv_all.at[pl.ds(0, 3), pl.ds(0, own)], wsend.at[0])
+        if is_inner:
+            sent(dv_all.at[pl.ds(0, 3), pl.ds(0, 3 * rows)], wsend.at[1])
+        for to_inner in (False, True):
+            size = part(to_inner)[1]
+            count = piece * (1 if to_inner == is_inner else 2)
+            for n in (0, 2):
+                sent(ex_all.at[pl.ds(0, count), pl.ds(0, size)], csend.at[n + int(to_inner)])
+
+    both(few_sent)
+    sent(dv_all.at[pl.ds(0, 3), pl.ds(0, 2 * rows)], xsend.at[0])
+    sent(mg_all.at[pl.ds(0, 3), pl.ds(0, rows)], xsend.at[1])
+    sent(xg.at[pl.ds(0, 3 * rows)], gsend.at[0])
+    sent(stat.at[pl.ds(0, 3)], gsend.at[1])
+    sent(r1, msend.at[0])
+    sent(s1, msend.at[1])
+    sent(nm.at[pl.ds(0, 7)], nsend.at[0])
+    over_fs.wait_send()
+    for n, ref in enumerate((r2, f1, f2, f3)):
+        sent(ref, fsend.at[n])
+    pltpu.make_async_copy(result, out_ref, out_sem).wait()
 
 
 def fused_body(
@@ -809,10 +862,10 @@
     return pl.pallas_call(
         fused_kernel,
         out_shape=jax.ShapeDtypeStruct((rows, width), bf),
-        in_specs=[pl.BlockSpec(memory_space=pltpu.VMEM)] * len(small)
-        + [pl.BlockSpec(memory_space=pl.ANY)] * len(large),
-        out_specs=pl.BlockSpec(memory_space=pltpu.VMEM),
-        scratch_shapes=[
+        in_specs=[pl.BlockSpec(memory_space=pl.ANY)] * len(small + large),
+        out_specs=pl.BlockSpec(memory_space=pl.ANY),
+        scratch_shapes=[vm(a.shape, a.dtype) for a in small]
+        + [
             vm((2, piece, local), f32),
             vm((local, piece), f32),
             vm((piece, wide), f32),
@@ -842,15 +895,15 @@
             vm((16, rows, thin), bf),
             vm((8, rows, thin), bf),
             vm((8, rows, thin), bf),
-            dma((5,)),
-            dma((3, 2, 3)), dma((3, 2, 3)),
-            dma((3, 2, 3)), dma((3, 2, 3)),
-            dma((10,)), dma((10,)),
-            dma((3,)), dma((3,)),
-            dma((3,)), dma((3,)),
-            dma((4, 2)), dma((4, 2)),
-            dma((21,)), dma((21,)),
-            dma((4, 16)), dma((4, 16)),
+            vm((rows, width), bf),
+            dma((17,)), dma,
+            dma((2,)), dma((3, 4)),
+            dma((2,)), dma((3, 4)),
+            dma((4,)), dma((7,)),
+            dma((2,)), dma((3,)), dma((3,)),
+            dma((2,)), dma((4, 2)),
+            dma((2,)), dma((21,)),
+            dma((4,)), dma((4, 16)),
         ],
         compiler_params=pltpu.CompilerParams(
             collective_id=0, has_side_effects=True, vmem_limit_bytes=62 * 1024 * 1024

time: 140 us -> 135 us (0.964)
  Pallas kernels: 138 us -> 133 us
    pallas_call x1, Pallas kernels: 138 us -> 133 us  [fused_body(): pl.pallas_call(fused_kernel, out_shape=jax.ShapeDtypeStruct((rows, width)...]
where the time goes in v3:
time: 135 us
  Pallas kernels  133 us (99%)
  local copies, waits for them, and re-layouts  1.88 us (1%)
    pallas_call x1, Pallas kernels, fused_body(): pl.pallas_call(fused_kernel, out_shape=jax.ShapeDtypeStruct((rows, width)...  133 us

profile of v3, /device:TPU:0, one launch (start us, length us, event | category | flops | bytes accessed | tf_op | source)
XLA Modules:
  0.0 135.2 jit_solution(13711465409031547355)
XLA Ops:
  0.0 133.3 %shard_map.163 = bf16[128,2048]{1,0:T(8,128)(2,1)} custom-call(bf16[128,2048]{1,0:T(8,128)(2,1)} %tok_hbm.1, f32[1,2048]{1,0:T(1,128)} %bitcast.9, f32[1,256]{1,0:T(1,128)} %bitcast.14, f32[1,256]{1,0:T(1,128)} %bitcast.15, f32[1,256]{1,0:T(1,128)} %bitcast.16, f32[1,256]{1,0:T(1,128)} %bitcast.17, bf16[4,128,128]{2,1,0:T(8,128)(2,1)} %sw_hbm.1, ...), custom_call_target="tpu_custom_call" | custom-call | tf_op jit(solution)/shard_map/pallas_call | solution.py:862
  133.3 1.9 %copy.19 = bf16[128,2048]{1,0:T(8,128)(2,1)} copy(bf16[128,2048]{1,0:T(8,128)(2,1)} %shard_map.163) | data formatting | bytes 1048576

commit v4 on v3

--- a/solution.py
+++ b/solution.py
@@ -185,9 +185,12 @@
             device_id=dev, device_id_type=MESH,
         )
 
+    quarters = 2 * rows // half
+    merge_item = quarters
+
     def item(i, slot, q):
-        if i < 2:
-            return dv_all.at[slot, span(q * 2 * rows + i * rows, rows)]
+        if i < quarters:
+            return dv_all.at[slot, span(q * 2 * rows + i * half, half)]
         return mg_all.at[slot, span(q * rows, rows)]
 
     def origin(way, d):
@@ -212,7 +215,7 @@
     def over(i, way, d):
         slot = origin(way, d)
         ref = item(i, slot, r)
-        return rcopy(ref, ref, xsend.at[i // 2], xrecv.at[i, slot], xnb)
+        return rcopy(ref, ref, xsend.at[i // quarters], xrecv.at[i, slot], xnb)
 
     def relay(i, d):
         for way in range(2):
@@ -227,6 +230,10 @@
                 @pl.when(jnp.logical_and(comes(way, d), goes(way)))
                 def _(way=way):
                     hop(i, way, d).start()
+
+    def relay_all(d):
+        for i in range(quarters):
+            relay(i, d)
 
     def over_wait(i, d):
         for way in range(2):
@@ -256,11 +263,15 @@
         for h in which:
             ex_copy(j, to_inner, h).start()
 
+    left, right, third_lanes, fourth_lanes = range(4)
+    lane_cuts = ((0, thin), (thin, thin), (thin, thin // 2), (thin + thin // 2, thin // 2))
+
     def rd_copy(side, j, to_inner, index=None):
         first, size = part(to_inner)
+        cut = pl.ds(*lane_cuts[side])
         n = 1 + side * 3 + (j if index is None else index)
         return rcopy(
-            rd_own.at[side, pl.ds(first, size)], rd_all.at[f, side, pl.ds(0, size)],
+            rd_own.at[pl.ds(first, size), cut], rd_all.at[f, pl.ds(0, size), cut],
             csend.at[2 + int(to_inner)], crecv.at[n], {"fs": peers[j]},
         )
 
@@ -298,7 +309,7 @@
         rcopy(far, far, gsend.at[0], grecv.at[2], sib),
     )
     pl.semaphore_wait(barrier, 6)
-    for i in range(2):
+    for i in range(quarters):
         for way in range(2):
 
             @pl.when(goes(way))
@@ -313,58 +324,51 @@
     loads[6].wait()
     ex_own[...] = ex_f32[...].astype(jnp.bfloat16)
 
-    relay(0, 1)
-    relay(1, 1)
+    relay_all(1)
     for way in range(2):
 
         @pl.when(inward(way))
         def _(way=way):
-            hop(2, way, 0).start()
+            hop(merge_item, way, 0).start()
 
     @pl.when(outer)
     def _():
         ex_start(0, True)
 
-    relay(0, 2)
-    relay(1, 2)
+    relay_all(2)
     for way in range(2):
 
         @pl.when(jnp.logical_and(jnp.logical_not(inward(way)), goes(way)))
         def _(way=way):
-            hop(2, way, 0).start()
+            hop(merge_item, way, 0).start()
 
     gather[1].wait_recv()
     gather[2].start()
 
     @pl.when(inner)
     def _():
-        relay(2, 1)
-        relay(2, 2)
+        relay(merge_item, 1)
+        relay(merge_item, 2)
         ex_start(2, True, (0,))
 
     @pl.when(outer)
     def _():
-        relay(0, 3)
-        relay(1, 3)
+        relay_all(3)
 
     for load in loads[7:]:
         load.wait()
-    for side in range(2):
-        cut = slice(side * thin, (side + 1) * thin)
-        rd_own[side] = (rd_f32[:, cut] * rscale_ref[:, cut]).astype(jnp.bfloat16)
+    rd_own[...] = (rd_f32[...] * rscale_ref[...]).astype(jnp.bfloat16)
 
     @pl.when(outer)
     def _():
         ex_all[:, small:] = jnp.zeros((width, big - small), jnp.bfloat16)
         for slot in range(4):
-            for side in range(2):
-                rd_all[slot, side, small:] = jnp.zeros((big - small, thin), jnp.bfloat16)
+            rd_all[slot, small:] = jnp.zeros((big - small, piece), jnp.bfloat16)
 
     def place_own(is_inner):
         first, size = part(is_inner)
         ex_all[columns(f), :size] = ex_own[:, first : first + size]
-        for side in range(2):
-            rd_all[f, side, :size] = rd_own[side, first : first + size]
+        rd_all[f, :size] = rd_own[first : first + size]
 
     both(place_own)
 
@@ -376,7 +380,7 @@
     act[...] = project(f)
 
     def project_more(d):
-        for i in range(2):
+        for i in range(quarters):
             over_wait(i, d)
         for way in range(2):
 
@@ -391,8 +395,8 @@
     @pl.when(outer)
     def _():
         ex_start(1, True, (0, 1))
-        relay(2, 1)
-        relay(2, 2)
+        relay(merge_item, 1)
+        relay(merge_item, 2)
 
     dvscale = jnp.concatenate([dscale_ref[...], vscale_ref[...]], axis=1)
     act[...] = jax.nn.gelu(act[...] * dvscale)
@@ -432,7 +436,7 @@
     @pl.when(outer)
     def _():
         ex_start(2, False)
-        relay(2, 3)
+        relay(merge_item, 3)
 
     inverse = 1.0 / (local * 4)
     group_lane = lax.broadcasted_iota(jnp.int32, (rows, 128), 1) // GDIM
@@ -481,20 +485,20 @@
 
     for k, slot in enumerate(merge_order):
         if k == 1:
-            over_wait(2, 1)
+            over_wait(merge_item, 1)
         if k == 2:
 
             @pl.when(outer)
             def _():
-                over_wait(2, 2)
+                over_wait(merge_item, 2)
 
         if k == 3:
 
             @pl.when(inner)
             def _():
-                over_wait(2, 2)
-
-            over_wait(2, 3)
+                over_wait(merge_item, 2)
+
+            over_wait(merge_item, 3)
         p1[k] = jnp.dot(gated[...], mg_all[slot], preferred_element_type=jnp.float32).astype(
             jnp.bfloat16
         )
@@ -591,15 +595,15 @@
 
     @pl.when(inner)
     def _():
-        for side in range(2):
+        for side in (left, right):
             rd_start(side, 0, False)
-        for side in range(2):
+        for side in (left, third_lanes, fourth_lanes):
             rd_start(side, 2, True)
             rd_start(side, 1, False)
 
     @pl.when(outer)
     def _():
-        for side in range(2):
+        for side in (left, right):
             rd_start(side, 0, True)
 
     fourth(near)
@@ -631,93 +635,120 @@
     def pick(if_inner, if_outer):
         return jnp.where(inner, if_inner, if_outer)
 
-    slots = (f, f, mate, mate, second_slot, last_slot, last_slot, second_slot)
-    sides = (0, 1, 0, 1, 0, 0, 1, 1)
-    came = (None, None, 0, 0, pick(2, 1), pick(1, 2), pick(1, 2), pick(2, 1))
+    slots = (f, f, mate, mate, second_slot, last_slot, last_slot, second_slot, second_slot)
+    sides = (left, right, left, right, left, left, right, third_lanes, fourth_lanes)
+    runs = (0, 0, 1, 1, 2, 3, 3, 2, 2)
+    came = (None, None, 0, 0, pick(2, 1), pick(1, 2), pick(1, 2), pick(2, 1), pick(2, 1))
     near_half, far_half = 0, 1
     units = tuple((k, h) for h in range(2) for k in range(4))
-    units += tuple((k, h) for k in range(4, 8) for h in (1, 0))
+    units += tuple((k, h) for k in range(4, len(slots)) for h in (1, 0))
 
     def plane(h):
         return z if h == near_half else 1 - z
 
     def arrived(side, j):
         both(lambda is_inner: rd_copy(side, 0, is_inner, j).wait_recv())
+
+    starts = tuple(run * piece + lane_cuts[side][0] for run, side in zip(runs, sides))
+
+    def lanes(k):
+        return slice(starts[k], starts[k] + lane_cuts[sides[k]][1])
 
     def reduce(u):
         k, h = units[u]
         slot, side = slots[k], sides[k]
+        first, size = lane_cuts[side]
         if k > 1 and h == (near_half if k < 4 else far_half):
             arrived(side, came[k])
         zz = plane(h)
 
         def step(i, _):
             g = zz * 4 + i * 2
-            p2[k, pl.ds(g, 2)] = (
+            p2[pl.ds(g, 2), :, :, lanes(k)] = (
                 jnp.dot(
-                    hid[pl.ds(g, 2)].reshape(2 * tall, big), rd_all[slot, side],
+                    hid[pl.ds(g, 2)].reshape(2 * tall, big),
+                    rd_all[slot, :, first : first + size],
                     preferred_element_type=jnp.float32,
                 )
                 .astype(jnp.bfloat16)
-                .reshape(2, 2, rows, thin)
+                .reshape(2, 2, rows, size)
             )
 
         lax.fori_loop(0, 2, step, None)
         pair(u).start()
+
+    y_first = tuple(u % 2 == 0 for u in range(len(units)))
+
+    def cols(k):
+        return pl.ds(lanes(k).start, lanes(k).stop - lanes(k).start)
 
     def pair(u):
         k, h = units[u]
         at = pl.ds(plane(h) * 4, 4)
-        return rcopy(p2.at[k, at, 1 - c], r2.at[k, at], fsend.at[0], frecv.at[0, u], sib)
+        return rcopy(
+            p2.at[at, 1 - c, :, cols(k)], r2.at[at, :, cols(k)], fsend.at[0], frecv.at[0, u], sib
+        )
 
     def summed_pair(k, g):
-        return p2[k, g, c].astype(jnp.float32) + r2[k, g].astype(jnp.float32)
+        return p2[g, c, :, lanes(k)].astype(jnp.float32) + r2[g, :, lanes(k)].astype(jnp.float32)
 
     def hop_one(u):
+        k, h = units[u]
+        at = (h, slice(None), slice(None), cols(k))
         return rcopy(
-            f1.at[u], a1.at[u], fsend.at[1], frecv.at[1, u], (ynb, xnb)[u % 2]
+            f1.at[at], a1.at[at], fsend.at[1], frecv.at[1, u], ynb if y_first[u] else xnb
         )
 
     def hop_two(u):
+        k, h = units[u]
+        at = (h, slice(None), cols(k))
         return rcopy(
-            f2.at[u], a2.at[u], fsend.at[2], frecv.at[2, u], (xnb, ynb)[u % 2]
-        )
+            f2.at[at], a2.at[at], fsend.at[2], frecv.at[2, u], xnb if y_first[u] else ynb
+        )
+
+    def lane_span(k):
+        first, size = lane_cuts[sides[k]]
+        return pl.ds(pl.multiple_of(slots[k] * piece + first, rows), size)
 
     def hop_three(k):
-        q = slots[k] * 2 + sides[k]
-        return rcopy(f3.at[k], a3.at[q], fsend.at[3], frecv.at[3, q], znb)
+        q = slots[k] * 4 + sides[k]
+        return rcopy(
+            f3.at[:, cols(k)], a3.at[:, lane_span(k)], fsend.at[3], frecv.at[3, q], znb
+        )
 
     def send_one(u):
         k, h = units[u]
         zz = plane(h)
         pair(u).wait_recv()
         for n in range(2):
-            g = group(zz, n, 1 - y) if u % 2 == 0 else group(zz, 1 - r, n)
-            f1[u, n] = summed_pair(k, g).astype(jnp.bfloat16)
+            g = group(zz, n, 1 - y) if y_first[u] else group(zz, 1 - r, n)
+            f1[h, n, :, lanes(k)] = summed_pair(k, g).astype(jnp.bfloat16)
         hop_one(u).start()
 
     def send_two(u):
         k, h = units[u]
         zz = plane(h)
         hop_one(u).wait_recv()
-        g, n = (group(zz, 1 - r, y), 1 - r) if u % 2 == 0 else (group(zz, r, 1 - y), 1 - y)
-        f2[u] = (summed_pair(k, g) + a1[u, n].astype(jnp.float32)).astype(jnp.bfloat16)
+        g, n = (group(zz, 1 - r, y), 1 - r) if y_first[u] else (group(zz, r, 1 - y), 1 - y)
+        f2[h, :, lanes(k)] = (
+            summed_pair(k, g) + a1[h, n, :, lanes(k)].astype(jnp.float32)
+        ).astype(jnp.bfloat16)
         hop_two(u).start()
 
     def own_sum(u):
         k, h = units[u]
-        n = r if u % 2 == 0 else y
+        n = r if y_first[u] else y
         hop_two(u).wait_recv()
         return (
             summed_pair(k, group(plane(h), r, y))
-            + a1[u, n].astype(jnp.float32)
-            + a2[u].astype(jnp.float32)
+            + a1[h, n, :, lanes(k)].astype(jnp.float32)
+            + a2[h, :, lanes(k)].astype(jnp.float32)
         )
 
     def send_three(u):
         k, h = units[u]
         if h == far_half:
-            f3[k] = own_sum(u).astype(jnp.bfloat16)
+            f3[:, lanes(k)] = own_sum(u).astype(jnp.bfloat16)
             hop_three(k).start()
 
     def ex_arrived(is_inner):
@@ -747,14 +778,15 @@
     away[8].wait_recv()
     expand(2, lambda i: jnp.where(i == 0, group(1 - z, 1 - r, y), group(1 - z, r, 1 - y)))
     once(send_one, 2)
+
+    @pl.when(outer)
+    def _():
+        rd_start(left, 2, False)
+        rd_start(left, 1, True)
+        rd_start(right, 1, True)
+        rd_start(right, 2, False)
+
     fourth(away)
-
-    @pl.when(outer)
-    def _():
-        for side in range(2):
-            rd_start(side, 2, False)
-            rd_start(side, 1, True)
-
     away[9].wait_recv()
     expand(1, lambda i: group(1 - z, 1 - r, 1 - y) + i)
     turn = (0, 1, 2, 4, 5, 3) + tuple(range(6, len(units)))
@@ -764,7 +796,7 @@
             once(action, turn[n])
 
     for n in range(3, len(turn)):
-        if n in (12, 14):
+        if n in (12, 14, 16):
             late(send_one, n - 1)
             late(send_two, n - 4)
             late(send_two, n - 3)
@@ -772,27 +804,23 @@
         late(send_one, n - 1)
         late(send_two, n - 4)
         late(send_three, n - 8)
-    once(send_one, 15)
-    once(send_two, 12)
-    once(send_three, 8)
-    once(send_two, 13)
-    once(send_three, 10)
-    once(send_two, 14)
-    once(send_three, 12)
-    once(send_two, 15)
-    once(send_three, 14)
+    count = len(units)
+    once(send_one, count - 1)
+    for u in range(count - 4, count):
+        once(send_two, u)
+        once(send_three, 2 * (u - 9))
+    once(send_three, count - 2)
 
     def stored(k):
-        at = span(slots[k] * piece + sides[k] * thin, thin)
+        at = lane_span(k)
         return pltpu.make_async_copy(result.at[:, at], out_ref.at[:, at], out_sem)
 
-    for k, (slot, side) in enumerate(zip(slots, sides)):
-        at = span(slot * piece + side * thin, thin)
+    for k in range(len(slots)):
+        at = lane_span(k)
         near_sum = own_sum(units.index((k, near_half)))
         hop_three(k).wait_recv()
-        q = slot * 2 + side
         result[:, at] = (
-            mid[:, at].astype(jnp.float32) + near_sum + a3[q].astype(jnp.float32)
+            mid[:, at].astype(jnp.float32) + near_sum + a3[:, at].astype(jnp.float32)
         ).astype(jnp.bfloat16)
         stored(k).start()
 
@@ -874,8 +902,8 @@
             vm((4, local, piece), bf),
             vm((4 * piece, big), bf),
             vm((piece, wide), bf),
-            vm((4, 2, big, thin), bf),
-            vm((2, wide, thin), bf),
+            vm((4, big, piece), bf),
+            vm((wide, piece), bf),
             vm((seq, width), bf),
             vm((seq, 2 * local), f32),
             vm((4, 4, 8, rows), f32),
@@ -887,23 +915,23 @@
             vm((rows, width), bf),
             vm((8, 2, rows, width), bf),
             vm((8, 2 * rows, big), bf),
-            vm((8, 8, 2, rows, thin), bf),
-            vm((8, 8, rows, thin), bf),
-            vm((16, 2, rows, thin), bf),
-            vm((16, 2, rows, thin), bf),
-            vm((16, rows, thin), bf),
-            vm((16, rows, thin), bf),
-            vm((8, rows, thin), bf),
-            vm((8, rows, thin), bf),
+            vm((8, 2, rows, width), bf),
+            vm((8, rows, width), bf),
+            vm((2, 2, rows, width), bf),
+            vm((2, 2, rows, width), bf),
+            vm((2, rows, width), bf),
+            vm((2, rows, width), bf),
+            vm((rows, width), bf),
+            vm((rows, width), bf),
             vm((rows, width), bf),
             dma((17,)), dma,
-            dma((2,)), dma((3, 4)),
-            dma((2,)), dma((3, 4)),
-            dma((4,)), dma((7,)),
+            dma((2,)), dma((5, 4)),
+            dma((2,)), dma((5, 4)),
+            dma((4,)), dma((13,)),
             dma((2,)), dma((3,)), dma((3,)),
             dma((2,)), dma((4, 2)),
             dma((2,)), dma((21,)),
-            dma((4,)), dma((4, 16)),
+            dma((4,)), dma((4, 18)),
         ],
         compiler_params=pltpu.CompilerParams(
             collective_id=0, has_side_effects=True, vmem_limit_bytes=62 * 1024 * 1024

time: 135 us -> 134 us (level)
  no operation moved by 1% of the time
where the time goes in v4:
time: 134 us
  Pallas kernels  132 us (99%)
  local copies, waits for them, and re-layouts  1.88 us (1%)
    pallas_call x1, Pallas kernels, fused_body(): pl.pallas_call(fused_kernel, out_shape=jax.ShapeDtypeStruct((rows, width)...  132 us

profile of v4, /device:TPU:0, one launch (start us, length us, event | category | flops | bytes accessed | tf_op | source)
XLA Modules:
  0.0 134.1 jit_solution(44961067239234611)
XLA Ops:
  0.0 132.2 %shard_map.163 = bf16[128,2048]{1,0:T(8,128)(2,1)} custom-call(bf16[128,2048]{1,0:T(8,128)(2,1)} %tok_hbm.1, f32[1,2048]{1,0:T(1,128)} %bitcast.9, f32[1,256]{1,0:T(1,128)} %bitcast.14, f32[1,256]{1,0:T(1,128)} %bitcast.15, f32[1,256]{1,0:T(1,128)} %bitcast.16, f32[1,256]{1,0:T(1,128)} %bitcast.17, bf16[4,128,128]{2,1,0:T(8,128)(2,1)} %sw_hbm.1, ...), custom_call_target="tpu_custom_call" | custom-call | tf_op jit(solution)/shard_map/pallas_call | solution.py:890
  132.2 1.9 %copy.19 = bf16[128,2048]{1,0:T(8,128)(2,1)} copy(bf16[128,2048]{1,0:T(8,128)(2,1)} %shard_map.163) | data formatting | bytes 1048576

commit v5 on v4

--- a/solution.py
+++ b/solution.py
@@ -348,8 +348,9 @@
     @pl.when(inner)
     def _():
         relay(merge_item, 1)
+        ex_start(2, True, (0, 1))
         relay(merge_item, 2)
-        ex_start(2, True, (0,))
+        ex_start(0, False, (0,))
 
     @pl.when(outer)
     def _():
@@ -395,8 +396,6 @@
     @pl.when(outer)
     def _():
         ex_start(1, True, (0, 1))
-        relay(merge_item, 1)
-        relay(merge_item, 2)
 
     dvscale = jnp.concatenate([dscale_ref[...], vscale_ref[...]], axis=1)
     act[...] = jax.nn.gelu(act[...] * dvscale)
@@ -417,6 +416,12 @@
     ]
     stats[1].start()
     stats[0].start()
+
+    @pl.when(outer)
+    def _():
+        relay(merge_item, 1)
+        relay(merge_item, 2)
+
     groups = sbias_ref.shape[0]
     down = lax.broadcasted_iota(jnp.int32, (rows, rows), 0)
     bias = jnp.zeros((rows, rows), jnp.float32)
@@ -431,7 +436,7 @@
     @pl.when(inner)
     def _():
         ex_start(1, False)
-        ex_start(2, True, (1, 2))
+        ex_start(2, True, (2,))
 
     @pl.when(outer)
     def _():
@@ -584,7 +589,7 @@
 
     @pl.when(inner)
     def _():
-        ex_start(0, False)
+        ex_start(0, False, (1, 2))
 
     third(near)
     over_fs.wait_recv()
@@ -635,10 +640,10 @@
     def pick(if_inner, if_outer):
         return jnp.where(inner, if_inner, if_outer)
 
-    slots = (f, f, mate, mate, second_slot, last_slot, last_slot, second_slot, second_slot)
-    sides = (left, right, left, right, left, left, right, third_lanes, fourth_lanes)
-    runs = (0, 0, 1, 1, 2, 3, 3, 2, 2)
-    came = (None, None, 0, 0, pick(2, 1), pick(1, 2), pick(1, 2), pick(2, 1), pick(2, 1))
+    slots = (f, f, mate, mate, second_slot) + (last_slot,) * 3 + (second_slot,) * 2
+    sides = (left, right, left, right, left, left) + (third_lanes, fourth_lanes) * 2
+    runs = (0, 0, 1, 1, 2, 3, 3, 3, 2, 2)
+    came = (None, None, 0, 0, pick(2, 1)) + (pick(1, 2),) * 3 + (pick(2, 1),) * 2
     near_half, far_half = 0, 1
     units = tuple((k, h) for h in range(2) for k in range(4))
     units += tuple((k, h) for k in range(4, len(slots)) for h in (1, 0))
@@ -658,7 +663,7 @@
         k, h = units[u]
         slot, side = slots[k], sides[k]
         first, size = lane_cuts[side]
-        if k > 1 and h == (near_half if k < 4 else far_half):
+        if k > 1 and h == (near_half if k < 5 else far_half):
             arrived(side, came[k])
         zz = plane(h)
 
@@ -764,8 +769,17 @@
 
     gathered(near)
     both(ex_arrived)
+
+    @pl.when(outer)
+    def _():
+        second(away)
+
     expand(4, lambda i: z * 4 + i)
-    second(away)
+
+    @pl.when(inner)
+    def _():
+        second(away)
+
     away[4].wait_recv()
     expand(1, lambda i: group(1 - z, r, y) + i)
     once(reduce, 0)
@@ -773,34 +787,37 @@
     third(away)
     once(send_one, 0)
     once(send_one, 1)
+
+    @pl.when(outer)
+    def _():
+        for side in (left, third_lanes, fourth_lanes):
+            rd_start(side, 2, False)
+            rd_start(side, 1, True)
+
     once(reduce, 2)
     away[7].wait_recv()
     away[8].wait_recv()
     expand(2, lambda i: jnp.where(i == 0, group(1 - z, 1 - r, y), group(1 - z, r, 1 - y)))
     once(send_one, 2)
-
-    @pl.when(outer)
-    def _():
-        rd_start(left, 2, False)
-        rd_start(left, 1, True)
-        rd_start(right, 1, True)
-        rd_start(right, 2, False)
-
     fourth(away)
+    once(reduce, 9)
     away[9].wait_recv()
+    once(send_one, 9)
     expand(1, lambda i: group(1 - z, 1 - r, 1 - y) + i)
-    turn = (0, 1, 2, 4, 5, 3) + tuple(range(6, len(units)))
+    turn = (0, 1, 2, 9, 4, 5, 3, 6, 7, 8) + tuple(range(10, len(units)))
 
     def late(action, n):
         if n >= 0:
             once(action, turn[n])
 
-    for n in range(3, len(turn)):
-        if n in (12, 14, 16):
+    for n in range(4, len(turn)):
+        if n in (10, 12, 14, 16, 18):
             late(send_one, n - 1)
             late(send_two, n - 4)
             late(send_two, n - 3)
         late(reduce, n)
+        if n == 5:
+            late(send_two, 1)
         late(send_one, n - 1)
         late(send_two, n - 4)
         late(send_three, n - 8)
@@ -808,8 +825,7 @@
     once(send_one, count - 1)
     for u in range(count - 4, count):
         once(send_two, u)
-        once(send_three, 2 * (u - 9))
-    once(send_three, count - 2)
+        once(send_three, 2 * (u - count // 2))
 
     def stored(k):
         at = lane_span(k)
@@ -931,7 +947,7 @@
             dma((2,)), dma((3,)), dma((3,)),
             dma((2,)), dma((4, 2)),
             dma((2,)), dma((21,)),
-            dma((4,)), dma((4, 18)),
+            dma((4,)), dma((4, 20)),
         ],
         compiler_params=pltpu.CompilerParams(
             collective_id=0, has_side_effects=True, vmem_limit_bytes=62 * 1024 * 1024

time: 134 us -> 131 us (0.978)
  Pallas kernels: 132 us -> 129 us
    pallas_call x1, Pallas kernels: 132 us -> 129 us  [fused_body(): pl.pallas_call(fused_kernel, out_shape=jax.ShapeDtypeStruct((rows, width)...]
where the time goes in v5:
time: 131 us
  Pallas kernels  129 us (98%)
  local copies, waits for them, and re-layouts  1.88 us (1%)
    pallas_call x1, Pallas kernels, fused_body(): pl.pallas_call(fused_kernel, out_shape=jax.ShapeDtypeStruct((rows, width)...  129 us

profile of v5, /device:TPU:0, one launch (start us, length us, event | category | flops | bytes accessed | tf_op | source)
XLA Modules:
  0.0 131.0 jit_solution(14289491486010609478)
XLA Ops:
  0.0 129.1 %shard_map.163 = bf16[128,2048]{1,0:T(8,128)(2,1)} custom-call(bf16[128,2048]{1,0:T(8,128)(2,1)} %tok_hbm.1, f32[1,2048]{1,0:T(1,128)} %bitcast.9, f32[1,256]{1,0:T(1,128)} %bitcast.14, f32[1,256]{1,0:T(1,128)} %bitcast.15, f32[1,256]{1,0:T(1,128)} %bitcast.16, f32[1,256]{1,0:T(1,128)} %bitcast.17, bf16[4,128,128]{2,1,0:T(8,128)(2,1)} %sw_hbm.1, ...), custom_call_target="tpu_custom_call" | custom-call | tf_op jit(solution)/shard_map/pallas_call | solution.py:906
  129.1 1.9 %copy.19 = bf16[128,2048]{1,0:T(8,128)(2,1)} copy(bf16[128,2048]{1,0:T(8,128)(2,1)} %shard_map.163) | data formatting | bytes 1048576

commit v6 on v5

--- a/solution.py
+++ b/solution.py
@@ -122,8 +122,8 @@
     dv_f32, mg_f32, ex_f32, rd_f32,
     dv_all, mg_all, ex_all, ex_own, rd_all, rd_own,
     xg, act, stat, gated, p1, r1, s1, x1, mid,
-    nm, hid, p2, r2, f1, a1, f2, a2, f3, a3, result,
-    load_sem, out_sem, wsend, wrecv, xsend, xrecv, csend, crecv, gsend, grecv, trecv, msend, mrecv,
+    nm, hid, p2, r2, f1, a1, f2, a2, f3, a3,
+    load_sem, wsend, wrecv, xsend, xrecv, csend, crecv, gsend, grecv, trecv, msend, mrecv,
     nsend, nrecv, fsend, frecv,
 ):
     rows, width = tok_ref.shape
@@ -827,18 +827,13 @@
         once(send_two, u)
         once(send_three, 2 * (u - count // 2))
 
-    def stored(k):
-        at = lane_span(k)
-        return pltpu.make_async_copy(result.at[:, at], out_ref.at[:, at], out_sem)
-
     for k in range(len(slots)):
         at = lane_span(k)
         near_sum = own_sum(units.index((k, near_half)))
         hop_three(k).wait_recv()
-        result[:, at] = (
+        out_ref[:, at] = (
             mid[:, at].astype(jnp.float32) + near_sum + a3[:, at].astype(jnp.float32)
         ).astype(jnp.bfloat16)
-        stored(k).start()
 
     def sent(ref, sem):
         rcopy(ref, ref, sem, crecv.at[0], znb).wait_send()
@@ -865,7 +860,6 @@
     over_fs.wait_send()
     for n, ref in enumerate((r2, f1, f2, f3)):
         sent(ref, fsend.at[n])
-    pltpu.make_async_copy(result, out_ref, out_sem).wait()
 
 
 def fused_body(
@@ -905,9 +899,9 @@
     large = (direct_weight, value_weight, merge_weight, expand_weight, reduce_weight)
     return pl.pallas_call(
         fused_kernel,
-        out_shape=jax.ShapeDtypeStruct((rows, width), bf),
+        out_shape=vm((rows, width), bf),
         in_specs=[pl.BlockSpec(memory_space=pl.ANY)] * len(small + large),
-        out_specs=pl.BlockSpec(memory_space=pl.ANY),
+        out_specs=pl.BlockSpec(memory_space=vm),
         scratch_shapes=[vm(a.shape, a.dtype) for a in small]
         + [
             vm((2, piece, local), f32),
@@ -939,8 +933,7 @@
             vm((2, rows, width), bf),
             vm((rows, width), bf),
             vm((rows, width), bf),
-            vm((rows, width), bf),
-            dma((17,)), dma,
+            dma((17,)),
             dma((2,)), dma((5, 4)),
             dma((2,)), dma((5, 4)),
             dma((4,)), dma((13,)),
@@ -950,7 +943,7 @@
             dma((4,)), dma((4, 20)),
         ],
         compiler_params=pltpu.CompilerParams(
-            collective_id=0, has_side_effects=True, vmem_limit_bytes=62 * 1024 * 1024
+            collective_id=0, has_side_effects=True, vmem_limit_bytes=60 * 1024 * 1024
         ),
     )(*small, *large)
 

time: 131 us -> 130 us (level)
  no operation moved by 1% of the time
where the time goes in v6:
time: 130 us; the launch traced here: 129 us
  Pallas kernels  129 us (99%)
    pallas_call x1, Pallas kernels, fused_body(): pl.pallas_call(fused_kernel, out_shape=vm((rows, width), bf), in_specs=[p...  129 us

profile of v6, /device:TPU:0, one launch (start us, length us, event | category | flops | bytes accessed | tf_op | source)
XLA Modules:
  0.0 129.4 jit_solution(9164828267599570429)
XLA Ops:
  0.0 128.6 %shard_map.163 = bf16[128,2048]{1,0:T(8,128)(2,1)S(1)} custom-call(bf16[128,2048]{1,0:T(8,128)(2,1)} %tok_hbm.1, f32[1,2048]{1,0:T(1,128)} %bitcast.9, f32[1,256]{1,0:T(1,128)} %bitcast.14, f32[1,256]{1,0:T(1,128)} %bitcast.15, f32[1,256]{1,0:T(1,128)} %bitcast.16, f32[1,256]{1,0:T(1,128)} %bitcast.17, bf16[4,128,128]{2,1,0:T(8,128)(2,1)} %sw_hbm.1, ...), custom_call_target="tpu_custom_call" | custom-call | tf_op jit(solution)/shard_map/pallas_call | solution.py:900
  128.6 0.8 copy.19
